TPU v7x, 512 devices: a whole 4x8x8 slice. The times are simulated.
512 devices in a mesh: sp: 64 (over z, y), tp: 8 (over x, core).
Axes of the slice: x: 4, y: 8, z: 8, core: 2. Of those that a mesh axis runs over, the one named last changes fastest.
Arguments:
- inner_pre: bfloat16 [24576, 4096], P('sp', 'tp'), may hold values from -6 to 6
- coeff_pre: bfloat16 [24576, 2, 1024], P('sp', None, 'tp'), may hold values from -6 to 6
- gate_pre: bfloat16 [24576, 4096], P('sp', 'tp'), may hold values from -6 to 6
- step_raw: bfloat16 [24576, 64], P('sp', 'tp'), may hold values from -2.5 to 2.5
- step_bias: float32 [64], P('tp'), may hold values from -3.3 to 0.8
- decay_log: float32 [64], P('tp'), may hold values from -8.5 to -3.5
- conv_inner: bfloat16 [4, 4096], P(None, 'tp'), may hold values from -3 to 3
- conv_coeff: bfloat16 [4, 2, 1024], P(None, None, 'tp'), may hold values from -3 to 3
- mixer_gain: float32 [4096], P('tp'), may hold values from 0.1 to 1.9
- out_weight: bfloat16 [4096, 2048], P('tp'), may hold values from -0.125 to 0.125
- residual: bfloat16 [24576, 2048], P('sp', 'tp'), may hold values from -12 to 12
- mlp_gain: float32 [2048], P('tp'), may hold values from 0.1 to 1.9
- up_weight: bfloat16 [2048, 8192], P('sp', 'tp'), may hold values from -0.125 to 0.125
- down_weight: bfloat16 [8192, 2048], P('tp', 'sp'), may hold values from -0.1875 to 0.1875
Outputs:
- layer_out: bfloat16 [24576, 2048], P('sp', 'tp')
All inputs are finite; a program needn't handle non-finite values.
Results may differ from a plain program's by a relative error of at most 0.02.
Values may be sent and summed in bfloat16 or wider, within the bound.
A program may use at most 64 MiB of HBM per device.

v0:
```python
import jax
import jax.numpy as jnp
from jax import lax
from jax.sharding import Mesh
from jax.sharding import PartitionSpec as P

D = 2048
INNER = 4096
HEAD_DIM = 64
GROUPS = 8
STATE = 128
BLOCK = 128
SP = ("sp_0", "sp_1")


eps_norm = 1e-05


def turned_gather(arrays, axis, dims):
    turned = [jnp.moveaxis(a, dim, 0) for a, dim in zip(arrays, dims)]
    both = jnp.concatenate([t.reshape(len(t), -1) for t in turned], axis=1)
    result, at, finished = (lax.all_gather(both, axis, axis=0, tiled=True), 0, [])
    for t, dim in zip(turned, dims):
        share = result[:, at : at + t[0].size].reshape(-1, *t.shape[1:])
        finished.append(jnp.moveaxis(share, 0, dim))
        at += t[0].size
    return tuple(finished)


def passed_along(block, axis, distance):
    devices = range(lax.axis_size(axis))
    route = [(i - distance, i) for i in devices if i - distance in devices]
    return lax.ppermute(block, axis, route)


def nothing_yet(array, identity):
    return jax.tree.map(
        lambda a, e: jnp.broadcast_to(jnp.asarray(e, a.dtype), a.shape), array, identity
    )


def carried_in(array, axes, combine, identity):
    before = start = nothing_yet(array, identity)
    so_far = array
    for axis in reversed(axes):
        size, index = (lax.axis_size(axis), lax.axis_index(axis))
        pieces = jax.tree.map(
            lambda part, kind: lax.all_gather(part.astype(kind), axis),
            so_far,
            (jnp.bfloat16, jnp.bfloat16),
        )
        inside, so_far = (start, start)
        for k in range(size):
            passed = k < index
            so_far = combine(
                so_far, jax.tree.map(lambda part, own: part[k].astype(own.dtype), pieces, array)
            )
            inside = jax.tree.map(lambda new, old: jnp.where(passed, new, old), so_far, inside)
        before = combine(inside, before)
    return before


def in_blocks(array, dim, size):
    before, after = (array.shape[:dim], array.shape[dim + 1 :])
    return jnp.moveaxis(array.reshape(*before, size, -1, *after), dim, 0)


def sent_and_summed(array, axis, dim):
    parts = in_blocks(array, dim, lax.axis_size(axis))
    arrived = lax.all_to_all(parts, axis, split_axis=0, concat_axis=0, tiled=True)
    return arrived.astype(jnp.float32).sum(axis=0)


def copy_for_each(array, axis):
    size = lax.axis_size(axis)
    return lax.all_to_all(
        jnp.broadcast_to(array[None], (size, *array.shape)), axis, 0, 0, tiled=True
    )


def of_everyone(array, axis):
    everything = copy_for_each(array, axis)
    return jnp.sum(everything, axis=0)


def laid_out(parts, dim):
    shape = list(parts.shape[1:])
    shape[dim] *= parts.shape[0]
    return jnp.moveaxis(parts, 0, dim).reshape(shape)


def gathered_copies(array, axis, dim):
    return laid_out(copy_for_each(array, axis), dim)


def causal_taps(history, current, weights):
    extended = jnp.concatenate([history, current], axis=0).astype(jnp.float32)
    length = current.shape[0]
    summed = extended[0:length] * weights[0].astype(jnp.float32)
    for offset in range(1, weights.shape[0]):
        summed = summed + extended[offset : offset + length] * weights[offset].astype(jnp.float32)
    return jax.nn.silu(summed)


def combine_states(first_part, second_part):
    decay_one, state_one = first_part
    decay_two, state_two = second_part
    return (decay_one * decay_two, state_one * decay_two[..., None, None] + state_two)


def shards(
    inner_pre,
    coeff_pre,
    gate_pre,
    step_raw,
    step_bias,
    decay_log,
    conv_inner,
    conv_coeff,
    mixer_gain,
    out_weight,
    residual,
    mlp_gain,
    up_weight,
    down_weight,
):
    up_whole, down_whole = turned_gather((up_weight, down_weight), SP, (0, 1))
    row_count = inner_pre.shape[0]
    edge_rows = conv_inner.shape[0] - 1
    inner_cols = inner_pre.shape[1]
    coeff_cols = coeff_pre.shape[2]
    tail_rows = jnp.concatenate(
        [
            inner_pre[row_count - edge_rows :],
            coeff_pre[row_count - edge_rows :].reshape(edge_rows, 2 * coeff_cols),
        ],
        axis=1,
    )
    arrived = passed_along(tail_rows, SP, 1)
    inner_act = causal_taps(arrived[:, :inner_cols], inner_pre, conv_inner)
    coeff_act = causal_taps(
        arrived[:, inner_cols:].reshape(edge_rows, 2, coeff_cols), coeff_pre, conv_coeff
    )
    heads_here = step_raw.shape[1]
    groups_here = coeff_cols // STATE
    per_group = heads_here // groups_here
    blocks = row_count // BLOCK
    in_coeff = coeff_act[:, 0].reshape(blocks, BLOCK, groups_here, STATE)
    out_coeff = coeff_act[:, 1].reshape(blocks, BLOCK, groups_here, STATE)
    step_size = jax.nn.softplus(step_raw.astype(jnp.float32) + step_bias)
    log_step = (-step_size * jnp.exp(decay_log)).reshape(blocks, BLOCK, groups_here, per_group)
    values = (
        inner_act.reshape(blocks, BLOCK, groups_here, per_group, HEAD_DIM)
        * step_size.reshape(blocks, BLOCK, groups_here, per_group)[..., None]
    )
    log_cumul = jnp.cumsum(log_step, axis=1)
    position = jnp.arange(BLOCK)
    causal_mask = (position[:, None] >= position[None, :])[None, :, :, None, None]
    log_gaps = log_cumul[:, :, None] - log_cumul[:, None, :]
    within = jnp.where(causal_mask, jnp.exp(jnp.where(causal_mask, log_gaps, 0.0)), 0.0)
    scores = jnp.einsum("blgn,bsgn->blsg", out_coeff, in_coeff)
    inside = jnp.einsum("blsg,blsgh,bsghp->blghp", scores, within, values)
    to_end = jnp.exp(log_cumul[:, -1:] - log_cumul)
    block_states = jnp.einsum("blgn,blgh,blghp->bghpn", in_coeff, to_end, values)
    block_logs = log_cumul[:, -1]
    block_ends = jnp.cumsum(block_logs, axis=0)
    block_starts = block_ends - block_logs
    block_index = jnp.arange(blocks)
    before = (block_index[None, :] < block_index[:, None])[:, :, None, None]
    log_spans = block_starts[:, None] - block_ends[None, :]
    block_links = jnp.where(before, jnp.exp(jnp.where(before, log_spans, 0.0)), 0.0)
    entering = jnp.einsum("nmgh,mghpk->nghpk", block_links, block_states)
    own_state = jnp.einsum(
        "mgh,mghpk->ghpk", jnp.exp(block_ends[-1][None] - block_ends), block_states
    )
    own_decay = jnp.exp(block_ends[-1])
    identity = (jnp.ones_like(own_decay), jnp.zeros_like(own_state))
    enter_decay, enter_state = carried_in((own_decay, own_state), SP, combine_states, identity)
    entering = entering + jnp.exp(block_starts)[..., None, None] * enter_state[None]
    carried = jnp.einsum("blgn,bghpn,blgh->blghp", out_coeff, entering, jnp.exp(log_cumul))
    scan_out = (inside + carried).reshape(row_count, inner_cols)
    gated = scan_out * jax.nn.silu(gate_pre.astype(jnp.float32))
    grouped = gated.reshape(row_count, groups_here, INNER // GROUPS)
    grouped = grouped * lax.rsqrt(jnp.mean(grouped * grouped, axis=2, keepdims=True) + eps_norm)
    mixed_rows = (grouped.reshape(row_count, inner_cols) * mixer_gain).astype(jnp.bfloat16)
    projected = sent_and_summed(
        jnp.dot(mixed_rows, out_weight, preferred_element_type=jnp.float32).astype(jnp.bfloat16),
        "tp",
        1,
    )
    first_sum = (residual.astype(jnp.float32) + projected).astype(jnp.bfloat16)
    first_wide = first_sum.astype(jnp.float32)
    squares = of_everyone(jnp.sum(first_wide * first_wide, axis=1), "tp")
    normed = (first_wide * lax.rsqrt(squares / D + eps_norm)[:, None] * mlp_gain).astype(
        jnp.bfloat16
    )
    whole_rows = gathered_copies(normed, "tp", 1)
    hidden = jnp.dot(whole_rows, up_whole, preferred_element_type=jnp.float32)
    active = jnp.square(jax.nn.relu(hidden)).astype(jnp.bfloat16)
    partials = jnp.dot(active, down_whole, preferred_element_type=jnp.float32)
    lowered = sent_and_summed(partials.astype(jnp.bfloat16), "tp", 1)
    return (first_wide + lowered).astype(jnp.bfloat16)


def solution(mesh):
    split = Mesh(mesh.devices.reshape(8, 8, mesh.shape["tp"]), ("sp_0", "sp_1", "tp"))
    return jax.shard_map(
        shards,
        mesh=split,
        in_specs=(
            P(SP, "tp"),
            P(SP, None, "tp"),
            P(SP, "tp"),
            P(SP, "tp"),
            P("tp"),
            P("tp"),
            P(None, "tp"),
            P(None, None, "tp"),
            P("tp"),
            P("tp", None),
            P(SP, "tp"),
            P("tp"),
            P(SP, "tp"),
            P("tp", SP),
        ),
        out_specs=P(SP, "tp"),
        check_vma=False,
    )
```

profile of v0, /device:TPU:1, one launch (start us, length us, event | category | flops | bytes accessed | tf_op | source)
XLA Modules:
  0.0 260.9 jit_solution(793769002312632758)
XLA Ops:
  6.5 0.9 slice.176
  7.4 0.7 slice_bitcast_fusion.8
  8.1 0.8 copy.96
  8.9 4.0 %collective-permute-start = (bf16[3,768]{0,1:T(8,128)(2,1)}, bf16[3,768]{0,1:T(8,128)(2,1)S(1)}, u32[]{:S(2)}, u32[]{:S(2)}) collective-permute-start(bf16[3,768]{0,1:T(8,128)(2,1)} %copy.96), channel_id=1, source_target_pairs={{0,8},{8,16},{16,24},{24,32},{32,40},{40,48},{48,56},{56,64},{64,7... | collective-permute-start | bytes 13832 | tf_op jit(solution)/shard_map/ppermute | solution.py:33
  13.0 0.7 exp.65
  13.6 0.8 fusion.70
  14.7 0.6 slice_bitcast_fusion.16
  15.3 0.6 bitcast_subtract_fusion
  15.9 0.8 slice_convert_fusion.3
  16.7 1.3 bitcast_convert_fusion.3
  18.1 0.7 fusion.99
  18.8 0.2 copy.102
  19.0 0.7 copy.106
  19.7 0.7 copy.122
  20.4 0.3 maximum_convert_fusion
  20.7 0.4 copy-done.11
  21.1 1.9 divide_multiply_fusion
  23.0 1.5 reshape.593
  24.6 1.1 maximum_convert_fusion.1
  25.8 0.6 divide_multiply_fusion.1
  26.4 0.3 fusion.98
  26.7 1.1 broadcast_multiply_fusion
  27.9 0.2 fusion.35
  28.2 0.4 fusion.24
  28.7 0.2 copy-done.9
  28.9 0.7 convert_element_type.466
  29.7 13.0 %all_gather.21 = bf16[8,1,8]{2,1,0:T(2,128)(2,1)S(1)} all-gather(bf16[1,1,8]{2,1,0:T(2,128)(2,1)S(1)} %copy-done.52), channel_id=1, replica_groups=mesh['sp_0'=8,'sp_1'=8,'tp'=8] {'sp_1'}, dimensions={0}, use_global_device_ids=true | all-gather | bytes 144 | tf_op jit(solution)/shard_map/all_gather | solution.py:48
  42.7 0.5 broadcast_select_fusion.7
  43.2 26.5 %all-gather.9.cloned.1.call-done = bf16[64,64,128]{2,1,0:T(8,128)(2,1)} async-done(((bf16[8,64,128]{2,1,0:T(8,128)(2,1)}), bf16[64,64,128]{2,1,0:T(8,128)(2,1)}) %all-gather.9.cloned.1.call-update) | async-done | bytes 1048592 | tf_op jit(solution)/shard_map/all_gather | solution.py:48
  69.7 2.2 fusion.64
  72.1 0.7 pad_maximum_fusion
  72.8 0.7 copy.100
  73.5 0.7 copy.112
  74.2 0.7 copy.125
  74.8 0.7 copy.110
  75.6 1.0 copy.115
  76.6 13.6 %all_gather.22 = bf16[8,1,8]{2,1,0:T(2,128)(2,1)S(1)} all-gather(bf16[1,1,8]{2,1,0:T(2,128)(2,1)S(1)} %multiply_convert_fusion.3), channel_id=1, replica_groups=mesh['sp_0'=8,'sp_1'=8,'tp'=8] {'sp_0'}, dimensions={0}, use_global_device_ids=true | all-gather | bytes 144 | tf_op jit(solution)/shard_map/all_gather | solution.py:48
  90.2 0.6 iota_compare_fusion.1
  90.8 0.6 iota_compare_fusion
  91.4 0.5 fusion.85
  91.9 0.6 fusion.83
  92.5 0.2 convolution_bitcast_fusion.1
  92.8 0.8 copy.98
  93.7 2.8 %fusion.17 = f32[3,128,1,8,64]{1,4,3,0,2:T(8,128)} fusion(bf16[3,128,8,64]{1,0,3,2:T(4,128)(2,1)} %get-tuple-element.8, f32[3,128,8]{1,2,0:T(8,128)} %copy.100, f32[3,128,128]{2,1,0:T(8,128)} %copy.98, pred[128,128]{1,0:T(8,128)(4,1)} %iota_compare_fusion), kind=kOutput, calls=%fused_computation.20 | convolution fusion | flops 51904512 | bytes 1404928 | tf_op jit(solution)/shard_map/blsg,blsgh,bsghp->blghp/dot_general | solution.py:162
  96.6 16.6 %all-gather.5.cloned.1.call-done = bf16[8,1,8,64,128]{4,3,2,1,0:T(8,128)(2,1)} async-done(((bf16[1,1,8,64,128]{4,3,2,1,0:T(8,128)(2,1)}), bf16[8,1,8,64,128]{4,3,2,1,0:T(8,128)(2,1)}) %all-gather.5.cloned.1.call-update) | async-done | bytes 1048592 | tf_op jit(solution)/shard_map/all_gather | solution.py:48
  113.4 2.0 fusion.63
  115.4 0.6 fusion.16
  116.1 0.5 copy-done.5
  116.5 0.3 fusion.21
  116.8 0.5 copy.114
  117.5 0.3 multiply_reduce_fusion
  117.8 1.2 convolution_convert_fusion
  119.1 29.9 %all_to_all.21 = bf16[8,384,256]{2,1,0:T(8,128)(2,1)S(1)} all-to-all(bf16[8,384,256]{2,1,0:T(8,128)(2,1)S(1)} %bitcast.260), channel_id=1, replica_groups=mesh['sp_0'=8,'sp_1'=8,'tp'=8] {'tp'}, dimensions={0} | all-to-all | bytes 3145728 | tf_op jit(solution)/shard_map/all_to_all | solution.py:70
  149.0 0.2 convert_reduce_fusion.1
  149.3 0.7 copy-done.12
  150.1 8.0 %all_to_all.22 = f32[8,1,384]{2,1,0:T(1,128)S(1)} all-to-all(f32[8,1,384]{2,1,0:T(1,128)S(1)} %broadcast_in_dim.53), channel_id=1, replica_groups=mesh['sp_0'=8,'sp_1'=8,'tp'=8] {'tp'}, dimensions={0} | all-to-all | bytes 24576 | tf_op jit(solution)/shard_map/all_to_all | solution.py:76
  158.3 0.2 copy.118
  158.7 24.4 %all_to_all.23 = bf16[8,384,256]{1,2,0:T(8,128)(2,1)} all-to-all(bf16[8,384,256]{1,2,0:T(8,128)(2,1)S(1)} %broadcast_in_dim.54), channel_id=1, replica_groups=mesh['sp_0'=8,'sp_1'=8,'tp'=8] {'tp'}, dimensions={0} | all-to-all | bytes 3145728 | tf_op jit(solution)/shard_map/all_to_all | solution.py:76
  183.1 34.8 %all-gather.7.cloned.1.call-done = bf16[2048,2048]{1,0:T(8,128)(2,1)} async-done(((bf16[32,2048]{1,0:T(8,128)(2,1)}), bf16[2048,2048]{1,0:T(8,128)(2,1)}) %all-gather.7.cloned.1.call-update) | async-done | bytes 8388624 | tf_op jit(solution)/shard_map/all_gather | solution.py:22
  217.9 8.5 %fusion.4 = bf16[384,2048]{1,0:T(8,128)(2,1)} fusion(bf16[2048,2048]{1,0:T(8,128)(2,1)} %all-gather.7.cloned.1.call-done, bf16[384,2048]{0,1:T(8,128)(2,1)} %bitcast.270), kind=kOutput, calls=%fused_computation.6 | convolution fusion | flops 3223191552 | bytes 11534336 | tf_op jit(solution)/shard_map/dot_general | solution.py:200
  226.4 1.5 copy.160
  227.9 25.5 %all_to_all.24 = bf16[8,384,256]{2,1,0:T(8,128)(2,1)S(1)} all-to-all(bf16[8,384,256]{2,1,0:T(8,128)(2,1)S(1)} %bitcast.261), channel_id=1, replica_groups=mesh['sp_0'=8,'sp_1'=8,'tp'=8] {'tp'}, dimensions={0} | all-to-all | bytes 3145728 | tf_op jit(solution)/shard_map/all_to_all | solution.py:70
  253.4 0.2 convert_reduce_fusion
  253.7 0.7 fusion.47
  (140 shorter events, 1.6 us)
Async XLA Ops:
  6.5 111.3 %copy-start = (bf16[512,2048]{1,0:T(8,128)(2,1)S(1)}, bf16[512,2048]{1,0:T(8,128)(2,1)}, u32[]{:S(2)}) copy-start(bf16[512,2048]{1,0:T(8,128)(2,1)} %param.23) | copy-start | bytes 6291460
  6.5 12.3 %copy-start.7 = (bf16[384,512]{1,0:T(8,128)(2,1)S(1)}, bf16[384,512]{1,0:T(8,128)(2,1)}, u32[]{:S(2)}) copy-start(bf16[384,512]{1,0:T(8,128)(2,1)} %param.14) | copy-start | bytes 1179652
  6.5 63.2 %all-gather.9.cloned.1.call-start = ((), (), s32[]{:S(2)}) async-start(), calls=%async_computation.6 | async-start | bytes 1179648 | tf_op jit(solution)/shard_map/all_gather | solution.py:48
  8.9 11.5 %collective-permute-start = (bf16[3,768]{0,1:T(8,128)(2,1)}, bf16[3,768]{0,1:T(8,128)(2,1)S(1)}, u32[]{:S(2)}, u32[]{:S(2)}) collective-permute-start(bf16[3,768]{0,1:T(8,128)(2,1)} %copy.96), channel_id=1, source_target_pairs={{0,8},{8,16},{16,24},{24,32},{32,40},{40,48},{48,56},{56,64},{64,7... | collective-permute-start | bytes 13832 | tf_op jit(solution)/shard_map/ppermute | solution.py:33
  14.7 4.1 %copy-start.16 = (f32[3,1,8]{2,1,0:T(1,128)}, f32[3,1,8]{2,1,0:T(1,128)S(1)}, u32[]{:S(2)}) copy-start(f32[3,1,8]{2,1,0:T(1,128)S(1)} %fusion.75) | copy-start | bytes 292
  15.9 2.2 copy-start.18
  20.4 0.7 copy-start.11
  23.0 1.5 slice-start
  23.0 2.7 %copy-start.35 = (f32[2,128]{1,0:T(2,128)S(1)}, f32[2,128]{1,0:T(2,128)}, u32[]{:S(2)}) copy-start(f32[2,128]{1,0:T(2,128)} %get-tuple-element.37) | copy-start | bytes 3076
  23.0 2.7 %copy-start.36 = (f32[2,128]{1,0:T(2,128)S(1)}, f32[2,128]{1,0:T(2,128)}, u32[]{:S(2)}) copy-start(f32[2,128]{1,0:T(2,128)} %get-tuple-element.38) | copy-start | bytes 3076
  23.0 2.7 %copy-start.37 = (f32[2,128]{1,0:T(2,128)S(1)}, f32[2,128]{1,0:T(2,128)}, u32[]{:S(2)}) copy-start(f32[2,128]{1,0:T(2,128)} %get-tuple-element.39) | copy-start | bytes 3076
  23.0 2.7 %copy-start.38 = (f32[2,128]{1,0:T(2,128)S(1)}, f32[2,128]{1,0:T(2,128)}, u32[]{:S(2)}) copy-start(f32[2,128]{1,0:T(2,128)} %get-tuple-element.40) | copy-start | bytes 3076
  24.6 2.1 copy-start.13
  26.7 1.9 copy-start.2
  26.7 1.4 copy-start.39
  27.9 1.8 copy-start.52
  28.1 0.8 copy-start.9
  28.1 43.9 %copy-start.14 = (bf16[1024,32]{0,1:T(8,128)(2,1)S(1)}, bf16[1024,32]{0,1:T(8,128)(2,1)}, u32[]{:S(2)}) copy-start(bf16[1024,32]{0,1:T(8,128)(2,1)} %param.27) | copy-start | bytes 196612
  28.2 43.9 %copy-start.15 = (bf16[32,1024]{1,0:T(8,128)(2,1)S(1)}, bf16[32,1024]{1,0:T(8,128)(2,1)}, u32[]{:S(2)}) copy-start(bf16[32,1024]{1,0:T(8,128)(2,1)} %param.26) | copy-start | bytes 196612
  28.2 44.6 %copy-start.17 = (f32[3,1,8]{2,1,0:T(1,128)S(1)}, f32[3,1,8]{2,1,0:T(1,128)}, u32[]{:S(2)}) copy-start(f32[3,1,8]{2,1,0:T(1,128)} %copy-done.16) | copy-start | bytes 292
  28.2 45.3 %copy-start.19 = (f32[3,1,1,8]{3,2,1,0:T(1,128)S(1)}, f32[3,1,1,8]{3,2,1,0:T(1,128)}, u32[]{:S(2)}) copy-start(f32[3,1,1,8]{3,2,1,0:T(1,128)} %copy-done.18) | copy-start | bytes 292
  28.2 46.0 %copy-start.20 = (f32[3,1,1,8]{3,2,1,0:T(1,128)S(1)}, f32[3,1,1,8]{3,2,1,0:T(1,128)}, u32[]{:S(2)}) copy-start(f32[3,1,1,8]{3,2,1,0:T(1,128)} %get-tuple-element.13) | copy-start | bytes 292
  28.2 47.3 %copy-start.6 = (f32[3,128,8]{2,1,0:T(8,128)S(1)}, f32[3,128,8]{2,1,0:T(8,128)}, u32[]{:S(2)}) copy-start(f32[3,128,8]{2,1,0:T(8,128)} %get-tuple-element.11) | copy-start | bytes 36868
  28.7 46.9 %copy-start.8 = (bf16[384,512]{1,0:T(8,128)(2,1)S(1)}, bf16[384,512]{1,0:T(8,128)(2,1)}, u32[]{:S(2)}) copy-start(bf16[384,512]{1,0:T(8,128)(2,1)} %param.16) | copy-start | bytes 1179652
  29.6 62.9 %copy-start.3 = (f32[384,1,128]{2,1,0:T(1,128)S(1)}, f32[384,1,128]{2,1,0:T(1,128)}, u32[]{:S(2)}) copy-start(f32[384,1,128]{2,1,0:T(1,128)} %copy-done.2) | copy-start | bytes 589828
  29.6 83.6 %all-gather.5.cloned.1.call-start = ((), (), s32[]{:S(2)}) async-start(), calls=%async_computation.4 | async-start | bytes 1179648 | tf_op jit(solution)/shard_map/all_gather | solution.py:48
  43.2 49.5 %copy-start.33 = (f32[8]{0:T(128)}, f32[8]{0:T(128)S(1)}, u32[]{:S(2)}) copy-start(f32[8]{0:T(128)S(1)} %get-tuple-element.25) | copy-start | bytes 100
  43.2 49.5 %copy-start.21 = (f32[8]{0:T(128)}, f32[8]{0:T(128)S(1)}, u32[]{:S(2)}) copy-start(f32[8]{0:T(128)S(1)} %get-tuple-element.27) | copy-start | bytes 100
  43.2 49.5 %copy-start.23 = (f32[8]{0:T(128)}, f32[8]{0:T(128)S(1)}, u32[]{:S(2)}) copy-start(f32[8]{0:T(128)S(1)} %get-tuple-element.28) | copy-start | bytes 100
  43.2 49.5 %copy-start.25 = (f32[8]{0:T(128)}, f32[8]{0:T(128)S(1)}, u32[]{:S(2)}) copy-start(f32[8]{0:T(128)S(1)} %get-tuple-element.29) | copy-start | bytes 100
  43.2 49.5 %copy-start.27 = (f32[8]{0:T(128)}, f32[8]{0:T(128)S(1)}, u32[]{:S(2)}) copy-start(f32[8]{0:T(128)S(1)} %get-tuple-element.30) | copy-start | bytes 100
  43.2 49.5 %copy-start.29 = (f32[8]{0:T(128)}, f32[8]{0:T(128)S(1)}, u32[]{:S(2)}) copy-start(f32[8]{0:T(128)S(1)} %get-tuple-element.31) | copy-start | bytes 100
  43.2 49.5 %copy-start.31 = (f32[8]{0:T(128)}, f32[8]{0:T(128)S(1)}, u32[]{:S(2)}) copy-start(f32[8]{0:T(128)S(1)} %get-tuple-element.32) | copy-start | bytes 100
  72.0 145.9 %all-gather.7.cloned.1.call-start = ((), (), s32[]{:S(2)}) async-start(), calls=%async_computation.5 | async-start | bytes 8519680 | tf_op jit(solution)/shard_map/all_gather | solution.py:22
  93.6 19.6 %copy-start.1 = (bf16[64,64,128]{2,1,0:T(8,128)(2,1)S(1)}, bf16[64,64,128]{2,1,0:T(8,128)(2,1)}, u32[]{:S(2)}) copy-start(bf16[64,64,128]{2,1,0:T(8,128)(2,1)} %all-gather.9.cloned.1.call-done) | copy-start | bytes 3145732
  93.6 19.6 %copy-start.22 = (f32[8]{0:T(128)S(1)}, f32[8]{0:T(128)}, u32[]{:S(2)}) copy-start(f32[8]{0:T(128)} %copy-done.21) | copy-start | bytes 100
  93.6 19.6 %copy-start.24 = (f32[8]{0:T(128)S(1)}, f32[8]{0:T(128)}, u32[]{:S(2)}) copy-start(f32[8]{0:T(128)} %copy-done.23) | copy-start | bytes 100
  93.6 19.6 %copy-start.26 = (f32[8]{0:T(128)S(1)}, f32[8]{0:T(128)}, u32[]{:S(2)}) copy-start(f32[8]{0:T(128)} %copy-done.25) | copy-start | bytes 100
  93.6 19.6 %copy-start.28 = (f32[8]{0:T(128)S(1)}, f32[8]{0:T(128)}, u32[]{:S(2)}) copy-start(f32[8]{0:T(128)} %copy-done.27) | copy-start | bytes 100
  93.6 19.6 %copy-start.30 = (f32[8]{0:T(128)S(1)}, f32[8]{0:T(128)}, u32[]{:S(2)}) copy-start(f32[8]{0:T(128)} %copy-done.29) | copy-start | bytes 100
  93.6 19.6 %copy-start.32 = (f32[8]{0:T(128)S(1)}, f32[8]{0:T(128)}, u32[]{:S(2)}) copy-start(f32[8]{0:T(128)} %copy-done.31) | copy-start | bytes 100
  93.6 19.6 %copy-start.34 = (f32[8]{0:T(128)S(1)}, f32[8]{0:T(128)}, u32[]{:S(2)}) copy-start(f32[8]{0:T(128)} %copy-done.33) | copy-start | bytes 100
  93.6 19.6 %copy-start.43 = (f32[8]{0:T(128)S(1)}, f32[8]{0:T(128)}, u32[]{:S(2)}) copy-start(f32[8]{0:T(128)} %get-tuple-element.17) | copy-start | bytes 100
  93.6 19.6 %copy-start.44 = (f32[8]{0:T(128)S(1)}, f32[8]{0:T(128)}, u32[]{:S(2)}) copy-start(f32[8]{0:T(128)} %get-tuple-element.18) | copy-start | bytes 100
  93.7 19.6 %copy-start.45 = (f32[8]{0:T(128)S(1)}, f32[8]{0:T(128)}, u32[]{:S(2)}) copy-start(f32[8]{0:T(128)} %get-tuple-element.19) | copy-start | bytes 100
  93.7 19.6 %copy-start.46 = (f32[8]{0:T(128)S(1)}, f32[8]{0:T(128)}, u32[]{:S(2)}) copy-start(f32[8]{0:T(128)} %get-tuple-element.20) | copy-start | bytes 100
  93.7 19.6 %copy-start.47 = (f32[8]{0:T(128)S(1)}, f32[8]{0:T(128)}, u32[]{:S(2)}) copy-start(f32[8]{0:T(128)} %get-tuple-element.21) | copy-start | bytes 100
  93.7 19.6 %copy-start.48 = (f32[8]{0:T(128)S(1)}, f32[8]{0:T(128)}, u32[]{:S(2)}) copy-start(f32[8]{0:T(128)} %get-tuple-element.22) | copy-start | bytes 100
  93.7 19.6 %copy-start.49 = (f32[8]{0:T(128)S(1)}, f32[8]{0:T(128)}, u32[]{:S(2)}) copy-start(f32[8]{0:T(128)} %get-tuple-element.23) | copy-start | bytes 100
  93.7 19.6 %copy-start.50 = (f32[8]{0:T(128)S(1)}, f32[8]{0:T(128)}, u32[]{:S(2)}) copy-start(f32[8]{0:T(128)} %get-tuple-element.24) | copy-start | bytes 100
  93.7 19.6 %copy-start.53 = (f32[8]{0:T(128)S(1)}, f32[8]{0:T(128)}, u32[]{:S(2)}) copy-start(f32[8]{0:T(128)} %fusion.85) | copy-start | bytes 100
  96.6 18.8 %copy-start.40 = (f32[3,8]{0,1:T(8,128)S(1)}, f32[3,8]{0,1:T(8,128)}, u32[]{:S(2)}) copy-start(f32[3,8]{0,1:T(8,128)} %copy.112) | copy-start | bytes 292
  96.6 18.8 %copy-start.41 = (f32[3,8]{0,1:T(8,128)S(1)}, f32[3,8]{0,1:T(8,128)}, u32[]{:S(2)}) copy-start(f32[3,8]{0,1:T(8,128)} %copy.110) | copy-start | bytes 292
  96.6 18.9 %copy-start.42 = (f32[3,1,1,8]{0,3,2,1:T(8,128)S(1)}, f32[3,1,1,8]{0,3,2,1:T(8,128)}, u32[]{:S(2)}) copy-start(f32[3,1,1,8]{0,3,2,1:T(8,128)} %copy.125) | copy-start | bytes 292
  96.6 18.9 %copy-start.55 = (pred[3,3]{1,0:T(4,128)(4,1)S(1)}, pred[3,3]{1,0:T(4,128)(4,1)}, u32[]{:S(2)}) copy-start(pred[3,3]{1,0:T(4,128)(4,1)} %iota_compare_fusion.1) | copy-start | bytes 31
  113.2 2.2 copy-start.10
  115.4 1.1 copy-start.5
  116.5 1.0 copy-start.4
  116.8 1.0 copy-start.54
  149.0 0.9 copy-start.12
  149.0 9.2 %copy-start.51 = (f32[256]{0:T(256)S(1)}, f32[256]{0:T(256)}, u32[]{:S(2)}) copy-start(f32[256]{0:T(256)} %param.25) | copy-start | bytes 3076
Sparse Core Ops, SparseCore 0:
  29.7 39.9 all-gather.8
  72.1 41.0 all-gather.4
  116.3 101.5 all-gather.6
where the time goes:
time: 262 us; the launch traced here: 261 us
  blocking collectives  115 us (44%)
  waiting for transfers between devices  78 us (30%)
  other arithmetic  20.3 us (8%)
  local copies, waits for them, and re-layouts  15.8 us (6%)
  matrix products  14.2 us (5%)
  between operations  14 us (5%)
  starting transfers between devices  4.1 us (2%)
    all_to_all x2, blocking collectives, sent_and_summed(): lax.all_to_all(parts, axis, split_axis=0, concat_axis=0, tiled=True)  55.5 us
    all_gather x2, waiting for transfers between devices, carried_in(): lax.all_gather(part.astype(kind), axis)  43.1 us
    all_gather x1, waiting for transfers between devices, turned_gather(): lax.all_gather(both, axis, axis=0, tiled=True)  34.8 us
    all_to_all x2, blocking collectives, copy_for_each(): lax.all_to_all(jnp.broadcast_to(array[None], (size, *array.shape)), axis,...  32.4 us
    all_gather x2, blocking collectives, carried_in(): lax.all_gather(part.astype(kind), axis)  26.6 us
    dot_general x1, matrix products, shards(): partials = jnp.dot(active, down_whole, preferred_element_type=jnp.float32)  8.49 us
  transfers between devices with their start and end apart: 4, of which 3 were waited for; matrix products, arithmetic and copies ran while one was open for 9% of the time, Pallas kernels for 0%

commit v1 on v0

v1 whole, which is shorter than its diff:
```python
import jax
import jax.numpy as jnp
from jax import lax
from jax.experimental import pallas as pl
from jax.experimental.pallas import tpu as pltpu
from jax.sharding import Mesh
from jax.sharding import PartitionSpec as P

MESH = pl.DeviceIdType.MESH
BF = jnp.bfloat16
F32 = jnp.float32
HIGH = lax.Precision.HIGHEST
EPS = 1e-05

ROWS = 384
HALF = ROWS // 2
BLOCK = 128
NB = ROWS // BLOCK
INNER = 512
STATE = 128
HEADS = 8
COLS = 256
FF = 1024
D = 2048
N = 8
NX = 4
PIECE = 32
SLICE = STATE // N
EDGE = 16


def dot(a, b, dims, precision=None):
    return lax.dot_general(a, b, (dims, ((), ())), precision=precision, preferred_element_type=F32)


NN = ((1,), (0,))
NT = ((1,), (1,))
TN = ((0,), (0,))


def per_head(v):
    low = lax.broadcasted_iota(jnp.int32, (v.shape[0], 128), 1) < 64
    tiles = [jnp.where(low, v[:, 2 * j : 2 * j + 1], v[:, 2 * j + 1 : 2 * j + 2]) for j in range(HEADS // 2)]
    return jnp.concatenate(tiles, axis=1)


def silu(v):
    return v / (1.0 + jnp.exp(-v))


def kernel(
    inner, coeff, gate, step_raw, step_bias, decay_log, taps_inner, taps_coeff, mixer_gain,
    out_hbm, residual, mlp_gain, up, down, result,
    hist_inner, hist_coeff, ext, act, cum, cum_t, step, step_t, local, states, own, enter,
    ld_own, ld_row, ld_total, ld_rows, pre, st_row, st_total, st_rows, st_back,
    mixed, out_w, up_all, down_all, gain_own, gain_all,
    pair_out, pair_in, far, relay_l, relay_r, near_l, near_r, keep_l, keep_r, fin_l, fin_r, keep,
    rows, first, acc, active,
    send, recv, w_send, w_recv, local_sem,
):
    z, y, x, c = (lax.axis_index(a) for a in ("z", "y", "x", "c"))
    tp = 2 * x + c
    at = lambda v, d: lax.rem(v + d, N)
    atx = lambda d: lax.rem(x + d, NX)
    next_id = {"z": at(z, jnp.where(y == N - 1, 1, 0)), "y": at(y, 1)}
    prev_id = {"z": at(z, jnp.where(y == 0, N - 1, 0)), "y": at(y, N - 1)}
    right, left = {"x": atx(1)}, {"x": atx(NX - 1)}
    partner = {"c": 1 - c}
    tp_id = lambda d: {"x": at(tp, d) // 2, "c": lax.rem(at(tp, d), 2)}

    barrier = pltpu.get_barrier_semaphore()
    greeted = [next_id, prev_id]
    for d in range(1, N):
        greeted += [{"y": at(y, d)}, {"z": at(z, d)}, tp_id(d)]
    for where in greeted:
        pl.semaphore_signal(barrier, inc=1, device_id=where, device_id_type=MESH)

    out_copy = pltpu.make_async_copy(out_hbm, out_w, local_sem)
    out_copy.start()

    started = []
    used = [0]

    def copy_to(src, dst, where, sems=None):
        if sems is None:
            sems = (send.at[used[0]], recv.at[used[0]])
            used[0] += 1
        copy = pltpu.make_async_remote_copy(
            src_ref=src, dst_ref=dst, send_sem=sems[0], recv_sem=sems[1], device_id=where, device_id_type=MESH
        )
        return copy

    def start(copy):
        copy.start()
        started.append(copy)
        return copy

    row_i = lax.broadcasted_iota(jnp.int32, (BLOCK, BLOCK), 0)
    col_i = lax.broadcasted_iota(jnp.int32, (BLOCK, BLOCK), 1)
    causal = row_i >= col_i
    tril = causal.astype(F32)
    triu = (row_i <= col_i).astype(F32)
    eye = (row_i == col_i).astype(F32)
    low_lanes = col_i < 64

    rate = jnp.exp(decay_log[...])
    ends = []
    for b in range(NB):
        rb = pl.ds(b * BLOCK, BLOCK)
        raw = step_raw[rb, :].astype(F32) + step_bias[...]
        size = jnp.maximum(raw, 0.0) + jnp.log1p(jnp.exp(-jnp.abs(raw)))
        logs = -size * rate
        cum_b = dot(tril, logs, NN, HIGH)
        cum[rb, :] = cum_b
        cum_t[:, rb] = dot(logs, triu, TN, HIGH)
        step[rb, :] = size
        step_t[:, rb] = dot(size, eye, TN, HIGH)
        ends.append(cum_b[BLOCK - 1 : BLOCK, :])
    total = ends[0] + ends[1] + ends[2]
    ld_own[...] = jnp.zeros_like(ld_own)
    ld_own[:, 0:HEADS] = jnp.broadcast_to(total, (8, HEADS))
    gain_own[...] = jnp.broadcast_to(mlp_gain[...], gain_own.shape)

    pl.semaphore_wait(barrier, len(greeted))

    tails = [
        start(copy_to(inner.at[pl.ds(ROWS - EDGE, EDGE)], hist_inner, next_id)),
        start(copy_to(coeff.at[pl.ds(ROWS - EDGE, EDGE)], hist_coeff, next_id)),
    ]
    ld_copies = [start(copy_to(ld_own, ld_row.at[y], {"y": at(y, d)})) for d in range(1, N)]
    gain_copies = [start(copy_to(gain_own, gain_all.at[tp], tp_id(d))) for d in range(1, N)]
    ld_row[y] = ld_own[...]
    gain_all[tp] = gain_own[...]

    first_up = [start(copy_to(up, up_all.at[z, y], {"z": at(z, d)})) for d in range(1, N)]
    first_down = [start(copy_to(down, down_all.at[z, y], {"y": at(y, d)})) for d in range(1, N)]
    up_all[z, y] = up[...]
    down_all[z, y] = down[...]

    def ring_copy(weight, way, hop, chunk):
        back = (N - (hop - 1)) % N if way == 0 else hop - 1
        part = pl.ds(4 * chunk, 4)
        if weight == 0:
            ref, where = up_all.at[part, at(y, back)], {"y": at(y, 1 if way == 0 else N - 1)}
        else:
            ref, where = down_all.at[at(z, back), part], {"z": at(z, 1 if way == 0 else N - 1)}
        i = ((weight * 2 + way) * 4 + hop - 1) * 2 + chunk
        return copy_to(ref, ref, where, (w_send.at[i], w_recv.at[i]))

    def ring_arrival(weight, way, hop, chunk):
        back = (N - hop) % N if way == 0 else hop
        part = pl.ds(4 * chunk, 4)
        if weight == 0:
            ref, where = up_all.at[part, at(y, back)], {"y": at(y, 1 if way == 0 else N - 1)}
        else:
            ref, where = down_all.at[at(z, back), part], {"z": at(z, 1 if way == 0 else N - 1)}
        i = ((weight * 2 + way) * 4 + hop - 1) * 2 + chunk
        copy_to(ref, ref, where, (w_send.at[i], w_recv.at[i])).wait_recv()

    def ring_first():
        for copy in first_up + first_down:
            copy.wait_recv()
        for chunk in range(2):
            for way in range(2):
                for weight in range(2):
                    start(ring_copy(weight, way, 1, chunk))

    def ring_next(hop, chunk):
        for way in range(2):
            for weight in range(2):
                ring_arrival(weight, way, hop - 1, chunk)
                start(ring_copy(weight, way, hop, chunk))

    def ring_last():
        for way in range(2):
            for weight in range(2):
                ring_arrival(weight, way, 3, way)
                start(ring_copy(weight, way, 4, way))

    def ring_end():
        for way in range(2):
            for weight in range(2):
                ring_arrival(weight, way, 3, 1 - way)
                ring_arrival(weight, way, 4, way)

    ext[8 : 8 + ROWS, 0:INNER] = inner[...].astype(F32)
    ext[8 : 8 + ROWS, INNER:] = coeff[...].astype(F32)

    def taps(b):
        for j in range(3):
            lanes = slice(COLS * j, COLS * (j + 1))
            weights = (taps_inner[:, lanes] if j < 2 else taps_coeff[...]).astype(F32)
            total_taps = ext[pl.ds(b * BLOCK + 5, BLOCK), lanes] * weights[0:1]
            for k in range(1, 4):
                total_taps = total_taps + ext[pl.ds(b * BLOCK + 5 + k, BLOCK), lanes] * weights[k : k + 1]
            act[b * BLOCK : (b + 1) * BLOCK, lanes] = silu(total_taps).astype(BF)

    def block_state(b):
        rb = slice(b * BLOCK, (b + 1) * BLOCK)
        weight = step[rb, :] * jnp.exp(ends[b] - cum[rb, :])
        values = act[rb, 0:INNER].astype(F32) * per_head(weight)
        states[b] = dot(act[rb, INNER : INNER + STATE], values.astype(BF), TN)

    taps(1)
    taps(2)
    block_state(1)
    block_state(2)
    for copy in tails:
        copy.wait_recv()
    is_first = jnp.logical_and(z == 0, y == 0)
    hist = jnp.concatenate([hist_inner[8:16, :].astype(F32), hist_coeff[8:16, :].astype(F32)], axis=1)
    ext[0:8, :] = jnp.where(is_first, 0.0, hist)
    taps(0)
    block_state(0)
    own[...] = (
        states[0] * per_head(jnp.exp(ends[1] + ends[2])) + states[1] * per_head(jnp.exp(ends[2])) + states[2]
    ).astype(BF)

    slice_of = lambda v: pl.ds(pl.multiple_of(v * SLICE, SLICE), SLICE)
    st1 = [start(copy_to(own.at[slice_of(at(y, d))], st_row.at[y], {"y": at(y, d)})) for d in range(1, N)]
    st_row[y] = own[slice_of(y), :]

    def inside(b):
        rb = slice(b * BLOCK, (b + 1) * BLOCK)
        scores = dot(act[rb, INNER + STATE :], act[rb, INNER : INNER + STATE], NT)
        for j in range(HEADS // 2):
            lanes = slice(128 * j, 128 * (j + 1))
            parts = []
            for h in (2 * j, 2 * j + 1):
                gap = cum[rb, h : h + 1] - cum_t[h : h + 1, rb]
                within = jnp.exp(jnp.where(causal, gap, -1e30)) * (scores * step_t[h : h + 1, rb])
                parts.append(dot(within.astype(BF), act[rb, lanes], NN))
            local[rb, lanes] = jnp.where(low_lanes, parts[0], parts[1])

    for copy in ld_copies:
        copy.wait_recv()
    row_logs = ld_row[:, 0, :]
    ld_total[...] = jnp.broadcast_to(jnp.sum(row_logs, axis=0, keepdims=True), (8, 128))
    ld2 = [start(copy_to(ld_total, ld_rows.at[z], {"z": at(z, d)})) for d in range(1, N)]
    ld_rows[z] = ld_total[...]
    row_decay = per_head(jnp.exp(row_logs))

    inside(0)
    for copy in st1:
        copy.wait_recv()
    run = jnp.zeros((SLICE, INNER), F32)
    for k in range(N):
        pre[k] = run
        run = run * row_decay[k : k + 1, :] + st_row[k].astype(F32)
    st_total[...] = run.astype(BF)
    st2 = [start(copy_to(st_total, st_rows.at[z], {"z": at(z, d)})) for d in range(1, N)]
    st_rows[z] = st_total[...]
    ring_first()
    inside(1)
    inside(2)
    for copy in ld2:
        copy.wait_recv()
    rows_decay = per_head(jnp.exp(ld_rows[:, 0, :]))
    for copy in st2:
        copy.wait_recv()
    run = jnp.zeros((SLICE, INNER), F32)
    for k in range(N):
        run = jnp.where(k < z, run * rows_decay[k : k + 1, :] + st_rows[k].astype(F32), run)
    for k in range(N):
        st_back[k] = (pre[k] + run).astype(BF)
        if k < N - 1:
            run = run * row_decay[k : k + 1, :]
    st3 = [
        start(copy_to(st_back.at[at(y, d)], enter.at[slice_of(y)], {"y": at(y, d)})) for d in range(1, N)
    ]
    enter[slice_of(y), :] = st_back[y]

    def carried(b):
        rb = slice(b * BLOCK, (b + 1) * BLOCK)
        if b == 1:
            inner_state = states[0]
        else:
            inner_state = states[0] * per_head(jnp.exp(ends[1])) + states[1]
        local[rb, :] += dot(act[rb, INNER + STATE :], inner_state.astype(BF), NN) * per_head(jnp.exp(cum[rb, :]))

    carried(1)
    carried(2)
    ring_next(2, 0)
    for copy in st3:
        copy.wait_recv()
    start_log = jnp.zeros_like(ends[0])
    for b in range(NB):
        rb = slice(b * BLOCK, (b + 1) * BLOCK)
        outer = dot(act[rb, INNER + STATE :], enter[...], NN) * per_head(jnp.exp(cum[rb, :] + start_log))
        gated = (local[rb, :] + outer) * silu(gate[rb, :].astype(F32))
        mean = jnp.mean(gated * gated, axis=1, keepdims=True)
        mixed[rb, :] = (gated * lax.rsqrt(mean + EPS) * mixer_gain[...]).astype(BF)
        start_log = start_log + ends[b]
    out_copy.wait()

    top, bottom = pl.ds(0, HALF), pl.ds(HALF, HALF)

    def reduced(block, use, pumps):
        pairs = []
        for i, dx in enumerate((2, 1, 3, 0)):
            pair_out[use, i] = block(2 * atx(dx) + 1 - c).astype(BF)
            pairs.append(start(copy_to(pair_out.at[use, i], pair_in.at[use, i], partner)))

        def mine(i, dx):
            value = block(2 * atx(dx) + c)
            pairs[i].wait_recv()
            return value + pair_in[use, i].astype(F32)

        far[use] = mine(0, 2).astype(BF)
        to_l = start(copy_to(far.at[use, top], relay_l.at[use], right))
        to_r = start(copy_to(far.at[use, bottom], relay_r.at[use], left))
        value = mine(1, 1)
        keep_r[...] = value[:HALF]
        near_r[use, HALF:, :] = value[HALF:].astype(BF)
        r_direct = start(copy_to(near_r.at[use, bottom], fin_l.at[use, bottom], right))
        value = mine(2, 3)
        keep_l[...] = value[HALF:]
        near_l[use, :HALF, :] = value[:HALF].astype(BF)
        l_direct = start(copy_to(near_l.at[use, top], fin_r.at[use, top], left))
        keep[...] = mine(3, 0)
        pumps[0]()
        to_l.wait_recv()
        near_r[use, :HALF, :] = (keep_r[...] + relay_l[use].astype(F32)).astype(BF)
        r_relay = start(copy_to(near_r.at[use, top], fin_l.at[use, top], right))
        to_r.wait_recv()
        near_l[use, HALF:, :] = (keep_l[...] + relay_r[use].astype(F32)).astype(BF)
        l_relay = start(copy_to(near_l.at[use, bottom], fin_r.at[use, bottom], left))
        pumps[1]()
        for copy in (r_direct, l_direct, r_relay, l_relay):
            copy.wait_recv()
        return keep[...] + fin_l[use].astype(F32) + fin_r[use].astype(F32)

    def out_block(owner):
        cols = pl.ds(pl.multiple_of(owner * COLS, COLS), COLS)
        return dot(mixed[...], out_w[:, cols], NN)

    projected = reduced(out_block, 0, (lambda: ring_next(2, 1), lambda: ring_next(3, 0)))
    first[...] = (residual[...].astype(F32) + projected).astype(BF)
    rows[tp] = first[...]

    mine_tp, left_tp, right_tp, far_tp = tp, 2 * atx(3) + c, 2 * atx(1) + c, 2 * atx(2) + c
    halves = {}
    halves["r0"] = start(copy_to(first.at[top], rows.at[tp, top], right))
    halves["l1"] = start(copy_to(first.at[bottom], rows.at[tp, bottom], left))
    across = [start(copy_to(first, rows.at[tp], partner))]
    halves["r1"] = start(copy_to(first.at[bottom], rows.at[tp, bottom], right))
    halves["l0"] = start(copy_to(first.at[top], rows.at[tp, top], left))
    for copy in gain_copies:
        copy.wait_recv()
    squares = jnp.zeros((ROWS, 1), F32)

    def raise_rows(source, squares, new=False):
        wide = rows[source].astype(F32)
        squares = squares + jnp.sum(wide * wide, axis=1, keepdims=True)
        scaled = (wide * gain_all[source][0:1, :]).astype(BF)
        weights = up_all[source].reshape(COLS, FF)
        product = dot(scaled, weights, NN)
        acc[...] = product if new else acc[...] + product
        return squares

    ring_next(3, 1)
    halves["r0"].wait_recv()
    fwd_r = start(copy_to(rows.at[left_tp, top], rows.at[left_tp, top], right))
    halves["l1"].wait_recv()
    fwd_l = start(copy_to(rows.at[right_tp, bottom], rows.at[right_tp, bottom], left))
    halves["r1"].wait_recv()
    across.append(start(copy_to(rows.at[left_tp], rows.at[left_tp], partner)))
    halves["l0"].wait_recv()
    across.append(start(copy_to(rows.at[right_tp], rows.at[right_tp], partner)))
    ring_last()
    fwd_r.wait_recv()
    fwd_l.wait_recv()
    across.append(start(copy_to(rows.at[far_tp], rows.at[far_tp], partner)))
    ring_end()
    squares = raise_rows(mine_tp, squares, True)
    squares = raise_rows(left_tp, squares)
    squares = raise_rows(right_tp, squares)
    squares = raise_rows(far_tp, squares)
    for copy, source in zip(across, (mine_tp, left_tp, right_tp, far_tp)):
        copy.wait_recv()
        squares = raise_rows(source + 1 - 2 * c, squares)
    scale = lax.rsqrt(squares * (1.0 / D) + EPS)
    active[...] = jnp.square(jnp.maximum(acc[...] * scale, 0.0)).astype(BF)

    def down_block(owner):
        return dot(active[...], down_all[owner].reshape(COLS, FF), NT)

    nothing = lambda: None
    lowered = reduced(down_block, 1, (nothing, nothing))
    result[...] = (first[...].astype(F32) + lowered).astype(BF)
    for copy in started:
        copy.wait_send()


def shards(
    inner_pre, coeff_pre, gate_pre, step_raw, step_bias, decay_log, conv_inner, conv_coeff, mixer_gain,
    out_weight, residual, mlp_gain, up_weight, down_weight,
):
    vm = pltpu.VMEM
    dma = pltpu.SemaphoreType.DMA
    in_vmem = pl.BlockSpec(memory_space=pltpu.VMEM)
    specs = [in_vmem] * 14
    specs[9] = pl.BlockSpec(memory_space=pl.ANY)
    scratch = [
        vm((EDGE, INNER), BF), vm((EDGE, COLS), BF), vm((ROWS + 8, INNER + COLS), F32), vm((ROWS, INNER + COLS), BF),
        vm((ROWS, HEADS), F32), vm((HEADS, ROWS), F32), vm((ROWS, HEADS), F32), vm((HEADS, ROWS), F32),
        vm((ROWS, INNER), F32), vm((NB, STATE, INNER), F32), vm((STATE, INNER), BF), vm((STATE, INNER), BF),
        vm((8, 128), F32), vm((N, 8, 128), F32), vm((8, 128), F32), vm((N, 8, 128), F32),
        vm((N, SLICE, INNER), F32), vm((N, SLICE, INNER), BF), vm((SLICE, INNER), BF), vm((N, SLICE, INNER), BF),
        vm((N, SLICE, INNER), BF),
        vm((ROWS, INNER), BF), vm((INNER, D), BF), vm((N, N, PIECE, FF), BF), vm((N, N, PIECE, FF), BF),
        vm((8, COLS), F32), vm((N, 8, COLS), F32),
        vm((2, NX, ROWS, COLS), BF), vm((2, NX, ROWS, COLS), BF), vm((2, ROWS, COLS), BF),
        vm((2, HALF, COLS), BF), vm((2, HALF, COLS), BF), vm((2, ROWS, COLS), BF), vm((2, ROWS, COLS), BF),
        vm((HALF, COLS), F32), vm((HALF, COLS), F32), vm((2, ROWS, COLS), BF), vm((2, ROWS, COLS), BF),
        vm((ROWS, COLS), F32),
        vm((N, ROWS, COLS), BF), vm((ROWS, COLS), BF), vm((ROWS, FF), F32), vm((ROWS, FF), BF),
        dma((96,)), dma((96,)), dma((32,)), dma((32,)), dma,
    ]
    return pl.pallas_call(
        kernel,
        out_shape=jax.ShapeDtypeStruct((ROWS, COLS), BF),
        in_specs=specs,
        out_specs=in_vmem,
        scratch_shapes=scratch,
        compiler_params=pltpu.CompilerParams(
            collective_id=0, has_side_effects=True, vmem_limit_bytes=60 * 1024 * 1024
        ),
        name="layer",
    )(
        inner_pre, coeff_pre.reshape(ROWS, COLS), gate_pre, step_raw, step_bias[None], decay_log[None], conv_inner,
        conv_coeff.reshape(4, COLS), mixer_gain[None], out_weight, residual, mlp_gain[None], up_weight, down_weight.T,
    )


def solution(mesh):
    split = Mesh(mesh.devices.reshape(N, N, NX, 2), ("z", "y", "x", "c"))
    sp, tp = ("z", "y"), ("x", "c")
    return jax.shard_map(
        shards,
        mesh=split,
        in_specs=(
            P(sp, tp), P(sp, None, tp), P(sp, tp), P(sp, tp), P(tp), P(tp), P(None, tp), P(None, None, tp), P(tp),
            P(tp, None), P(sp, tp), P(tp), P(sp, tp), P(tp, sp),
        ),
        out_specs=P(sp, tp),
        check_vma=False,
    )
```

time: 262 us -> 106 us (0.40)
  blocking collectives: 115 us -> 0 us
  Pallas kernels: 0 us -> 99.7 us
  waiting for transfers between devices: 78 us -> 0 us
  other arithmetic: 20.3 us -> 0 us
  matrix products: 14.2 us -> 0 us
  between operations: 14 us -> 0.01 us
  local copies, waits for them, and re-layouts: 15.8 us -> 5.98 us
  starting transfers between devices: 4.1 us -> 0 us
    pallas_call x0 -> x1, Pallas kernels: none -> 99.7 us  [shards(): pl.pallas_call(kernel, out_shape=jax.ShapeDtypeStruct((ROWS, COLS), BF),...]
    all_to_all x4 -> x0, blocking collectives: 87.9 us -> none  [the longest x2 55.5 us: sent_and_summed(): lax.all_to_all(parts, axis, split_axis=0, concat_axis=0, tiled=True)]
    all_gather x3 -> x0, waiting for transfers between devices: 78 us -> none  [the longest x2 43.1 us: carried_in(): lax.all_gather(part.astype(kind), axis)]
    all_gather x2 -> x0, blocking collectives: 26.6 us -> none  [carried_in(): lax.all_gather(part.astype(kind), axis)]
    dot_general x8 -> x0, matrix products: 14.2 us -> none  [the longest x1 8.49 us: shards(): partials = jnp.dot(active, down_whole, preferred_element_type=jnp.float32)]
    mul x6 -> x0, other arithmetic: 7.47 us -> none  [the longest x2 2.53 us: causal_taps(): return jax.nn.silu(summed)]
    convert_element_type x9 -> x0, other arithmetic: 5.8 us -> none  [the longest x3 2.93 us: carried_in(): part.astype(kind)]
    ppermute x1 -> x0, starting transfers between devices: 4.02 us -> none  [passed_along(): return lax.ppermute(block, axis, route)]
  transfers between devices with their start and end apart: 4 -> 0, of which waited for: 3 -> 0; matrix products, arithmetic and copies ran while one was open for 9% -> 0% of each run, Pallas kernels for 0% -> 0%
where the time goes in v1:
time: 106 us
  Pallas kernels  99.7 us (94%)
  local copies, waits for them, and re-layouts  5.98 us (6%)
    pallas_call x1, Pallas kernels, shards(): pl.pallas_call(kernel, out_shape=jax.ShapeDtypeStruct((ROWS, COLS), BF),...  99.7 us
    unnamed x4, local copies, waits for them, and re-layouts  5.98 us

profile of v1, /device:TPU:1, one launch (start us, length us, event | category | flops | bytes accessed | tf_op | source)
XLA Modules:
  0.0 105.7 jit_solution(14152644596288023575)
XLA Ops:
  0.0 1.3 %copy.21 = bf16[1,4,2,128]{3,1,2,0:T(4,128)(2,1)} copy(bf16[1,4,2,128]{3,2,1,0:T(2,128)(2,1)} %bitcast.18) | data formatting | bytes 4096
  1.3 1.5 %copy.15.step_raw = bf16[384,8]{1,0:T(8,128)(2,1)} copy(bf16[384,8]{0,1:T(8,128)(2,1)} %param.17) | data formatting | bytes 12288 | tf_op args[3]
  2.7 1.6 %copy.20 = bf16[48,8,2,128]{3,1,2,0:T(8,128)(2,1)} copy(bf16[48,8,2,128]{3,2,1,0:T(2,128)(2,1)} %bitcast.14) | data formatting | bytes 393216
  4.4 99.7 %layer.1 = bf16[384,256]{1,0:T(8,128)(2,1)} custom-call(bf16[384,512]{1,0:T(8,128)(2,1)} %inner.1, bf16[384,256]{1,0:T(8,128)(2,1)} %bitcast.13, bf16[384,512]{1,0:T(8,128)(2,1)} %gate.1, bf16[384,8]{1,0:T(8,128)(2,1)} %copy.15.step_raw, f32[1,8]{1,0:T(1,128)} %bitcast.20, f32[1,8]{1,0:T(1,128)} %bitcast.21, bf16[4,512]{1,0:T(4,128)(2,1)} %taps_inner.1, ...), custom_call_target="tpu_custom_call" | custom-call | tf_op jit(solution)/shard_map/layer/pallas_call | solution.py:420
  104.1 1.6 %copy.23 = bf16[384,256]{1,0:T(8,128)(2,1)} copy(bf16[384,256]{1,0:T(8,128)(2,1)} %layer.1) | data formatting | bytes 393216

commit v2 on v1

v2 whole, which is shorter than its diff:
```python
import jax
import jax.numpy as jnp
from jax import lax
from jax.experimental import pallas as pl
from jax.experimental.pallas import tpu as pltpu
from jax.sharding import Mesh
from jax.sharding import PartitionSpec as P

MESH = pl.DeviceIdType.MESH
BF = jnp.bfloat16
F32 = jnp.float32
HIGH = lax.Precision.HIGHEST
EPS = 1e-05

ROWS = 384
HALF = ROWS // 2
BLOCK = 128
NB = ROWS // BLOCK
INNER = 512
STATE = 128
HEADS = 8
COLS = 256
FF = 1024
D = 2048
N = 8
NX = 4
PIECE = 32
SLICE = STATE // N
EDGE = 16


def dot(a, b, dims, precision=None):
    return lax.dot_general(a, b, (dims, ((), ())), precision=precision, preferred_element_type=F32)


NN = ((1,), (0,))
NT = ((1,), (1,))
TN = ((0,), (0,))


def per_head(v):
    low = lax.broadcasted_iota(jnp.int32, (v.shape[0], 128), 1) < 64
    tiles = [jnp.where(low, v[:, 2 * j : 2 * j + 1], v[:, 2 * j + 1 : 2 * j + 2]) for j in range(HEADS // 2)]
    return jnp.concatenate(tiles, axis=1)


def silu(v):
    return v / (1.0 + jnp.exp(-v))


def kernel(
    inner_hbm, coeff_hbm, gate_hbm, step_raw, step_bias, decay_log, taps_inner, taps_coeff, mixer_gain,
    out_hbm, residual_hbm, mlp_gain, up_hbm, down_hbm, result,
    inner, coeff, gate, residual, up, down,
    hist_inner, hist_coeff, ext, ext_c, act, cum, cum_t, step, step_t, local, states, own, enter,
    ld_own, ld_row, ld_total, ld_rows, pre, st_row, st_total, st_rows, st_back,
    mixed, out_w, up_all, down_all, gain_own, gain_all,
    pair_out, pair_in, far, relay_l, relay_r, near_l, near_r, fin_l, fin_r, keep,
    rows, first, acc, active,
    send, recv, local_sem,
):
    z, y, x, c = (lax.axis_index(a) for a in ("z", "y", "x", "c"))
    tp = 2 * x + c
    at = lambda v, d: lax.rem(v + d, N)
    atx = lambda d: lax.rem(x + d, NX)
    next_id = {"z": at(z, jnp.where(y == N - 1, 1, 0)), "y": at(y, 1)}
    prev_id = {"z": at(z, jnp.where(y == 0, N - 1, 0)), "y": at(y, N - 1)}
    right, left = {"x": atx(1)}, {"x": atx(NX - 1)}
    partner = {"c": 1 - c}
    tp_id = lambda d: {"x": at(tp, d) // 2, "c": lax.rem(at(tp, d), 2)}

    barrier = pltpu.get_barrier_semaphore()
    greeted = [next_id, prev_id]
    for d in range(1, N):
        greeted += [{"y": at(y, d)}, {"z": at(z, d)}, tp_id(d)]
    for where in greeted:
        pl.semaphore_signal(barrier, inc=1, device_id=where, device_id_type=MESH)

    fetched = [
        pltpu.make_async_copy(there, here, local_sem.at[i])
        for i, (there, here) in enumerate(
            (
                (up_hbm, up), (down_hbm, down), (inner_hbm, inner), (coeff_hbm, coeff), (gate_hbm, gate),
                (residual_hbm, residual), (out_hbm, out_w),
            )
        )
    ]
    for copy in fetched:
        copy.start()
    up_copy, down_copy, inner_copy, coeff_copy, gate_copy, residual_copy, out_copy = fetched

    used = [0, 0]
    pending = []

    def remote(src, dst, where, sent, arrived):
        return pltpu.make_async_remote_copy(
            src_ref=src, dst_ref=dst, send_sem=sent, recv_sem=arrived, device_id=where, device_id_type=MESH
        )

    def sender(total):
        used[0] += 1
        pending.append((send.at[used[0] - 1], total))
        return send.at[used[0] - 1]

    def receiver():
        used[1] += 1
        return recv.at[used[1] - 1]

    def go(*args):
        remote(*args).start()

    def landed(arrived, total):
        remote(total, total, partner, send.at[0], arrived).wait_recv()

    row_i = lax.broadcasted_iota(jnp.int32, (BLOCK, BLOCK), 0)
    col_i = lax.broadcasted_iota(jnp.int32, (BLOCK, BLOCK), 1)
    causal = row_i >= col_i
    tril = causal.astype(F32)
    triu = (row_i <= col_i).astype(F32)
    eye = (row_i == col_i).astype(F32)
    low_lanes = col_i < 64

    on_heads = lax.broadcasted_iota(jnp.int32, (HEADS, HEADS), 0) == lax.broadcasted_iota(jnp.int32, (HEADS, HEADS), 1)
    column = lambda v: jnp.sum(jnp.where(on_heads, jnp.broadcast_to(v, (HEADS, HEADS)), 0.0), axis=1, keepdims=True)
    bias = column(step_bias[...])
    rate = jnp.exp(column(decay_log[...]))
    ends = []
    for b in range(NB):
        rb = pl.ds(b * BLOCK, BLOCK)
        raw = step_raw[:, rb].astype(F32) + bias
        size = jnp.maximum(raw, 0.0) + jnp.log1p(jnp.exp(-jnp.abs(raw)))
        logs = -size * rate
        cum_b = dot(tril, logs, NT, HIGH)
        cum[rb, :] = cum_b
        cum_t[:, rb] = dot(logs, triu, NN, HIGH)
        step[rb, :] = dot(eye, size, NT, HIGH)
        step_t[:, rb] = size
        ends.append(cum_b[BLOCK - 1 : BLOCK, :])
    total = ends[0] + ends[1] + ends[2]
    ld_own[...] = jnp.zeros_like(ld_own)
    ld_own[:, 0:HEADS] = jnp.broadcast_to(total, (8, HEADS))
    gain_own[...] = jnp.broadcast_to(mlp_gain[...], gain_own.shape)

    pl.semaphore_wait(barrier, len(greeted))

    inner_copy.wait()
    coeff_copy.wait()
    inner_tail, coeff_tail = receiver(), receiver()
    go(inner.at[pl.ds(ROWS - EDGE, EDGE)], hist_inner, next_id, sender(hist_inner), inner_tail)
    go(coeff.at[pl.ds(ROWS - 8, 8)], hist_coeff, next_id, sender(hist_coeff), coeff_tail)
    seven = pl.ds(0, N - 1)

    def to_all(source, target, where):
        sent, arrived = sender(target[1]), receiver()
        for d in range(1, N):
            go(source(d), target[0], where(d), sent, arrived)
        return lambda: landed(arrived, target[1])

    along_y, along_z = lambda d: {"y": at(y, d)}, lambda d: {"z": at(z, d)}
    ld_landed = to_all(lambda d: ld_own, (ld_row.at[y], ld_row.at[seven]), along_y)
    gain_landed = to_all(lambda d: gain_own, (gain_all.at[tp], gain_all.at[seven]), tp_id)
    ld_row[y] = ld_own[...]
    gain_all[tp] = gain_own[...]

    up_copy.wait()
    down_copy.wait()
    OFFSETS = ((0,), (N - 1, 1), (N - 2, 2), (N - 3, 3), (4,))
    weights_sent = [[sender(w.at[0, seven]), sender(w.at[seven])] for w in (up_all, down_all)]
    weights_landed = [
        [[receiver() for _ in range(4)], [[receiver() for _ in range(5)] for _ in range(4)]] for _ in range(2)
    ]

    def forward(weight, stage, way, hop, batch=0, offset=0):
        back = (N - (hop - 1)) % N if way == 0 else hop - 1
        to = 1 if way == 0 else N - 1
        a, b = (z, y) if weight == 0 else (y, z)
        a_axis, b_axis = ("z", "y") if weight == 0 else ("y", "z")
        arrived = weights_landed[weight][stage][hop - 1]
        if stage == 0:
            ia, ib, where = at(a, back), b, {a_axis: at(a, to)}
        else:
            ia, ib, where = at(a, offset), at(b, back), {b_axis: at(b, to)}
            arrived = arrived[batch]
        ref = up_all.at[ia, ib] if weight == 0 else down_all.at[ib, ia]
        source = ref
        if hop == 1 and offset == 0:
            source = up if weight == 0 else down
        if hop == 4:
            ref = source = ref.at[pl.ds(16 * way, 16)]
        go(source, ref, where, weights_sent[weight][stage], arrived)

    def pieces_landed(weight, stage, hop, batch=0):
        count = len(OFFSETS[batch]) * (1 if hop == 4 else 2)
        arrived = weights_landed[weight][stage][hop - 1]
        if stage == 0:
            arrived, count = arrived, 1 if hop == 4 else 2
        else:
            arrived = arrived[batch]
        landed(arrived, (up_all if weight == 0 else down_all).at[0, pl.ds(0, count)])

    def along(hop):
        for w in range(2):
            if hop > 1:
                pieces_landed(w, 0, hop - 1)
            if hop < 5:
                forward(w, 0, 0, hop)
                forward(w, 0, 1, hop)

    def across_to(hop, batch):
        for w in range(2):
            if hop > 1:
                pieces_landed(w, 1, hop - 1, batch)
            for offset in OFFSETS[batch]:
                forward(w, 1, 0, hop, batch, offset)
                forward(w, 1, 1, hop, batch, offset)

    def event(k):
        if k < 5:
            along(k + 1)
        for hop, batch in EVENTS[k]:
            across_to(hop, batch)

    EVENTS = (
        ((1, 0),),
        ((1, 1),),
        ((1, 2), (2, 0)),
        ((1, 3), (2, 1)),
        ((1, 4), (2, 2), (3, 0)),
        ((2, 3), (3, 1)),
        ((2, 4), (3, 2), (4, 0)),
        ((3, 3), (4, 1)),
        ((3, 4), (4, 2)),
        ((4, 3),),
        ((4, 4),),
    )
    event(0)
    up_all[z, y] = up[...]
    down_all[z, y] = down[...]

    ext[8 : 8 + ROWS, :] = inner[...].astype(F32)
    ext_c[8 : 8 + ROWS] = coeff[...].astype(F32)

    def taps(b):
        for j in range(4):
            if j < 2:
                lanes = slice(COLS * j, COLS * (j + 1))
                weights = taps_inner[:, lanes].astype(F32)
                shifted = lambda k: ext[pl.ds(b * BLOCK + 5 + k, BLOCK), lanes]
                target = lanes
            else:
                weights = taps_coeff[...].astype(F32)[:, j - 2, :]
                shifted = lambda k: ext_c[pl.ds(b * BLOCK + 5 + k, BLOCK), j - 2, :]
                target = slice(INNER + STATE * (j - 2), INNER + STATE * (j - 1))
            total_taps = shifted(0) * weights[0:1]
            for k in range(1, 4):
                total_taps = total_taps + shifted(k) * weights[k : k + 1]
            act[b * BLOCK : (b + 1) * BLOCK, target] = silu(total_taps).astype(BF)

    def block_state(b):
        rb = slice(b * BLOCK, (b + 1) * BLOCK)
        weight = step[rb, :] * jnp.exp(ends[b] - cum[rb, :])
        values = act[rb, 0:INNER].astype(F32) * per_head(weight)
        states[b] = dot(act[rb, INNER : INNER + STATE], values.astype(BF), TN)

    taps(1)
    taps(2)
    block_state(1)
    block_state(2)
    landed(inner_tail, hist_inner)
    landed(coeff_tail, hist_coeff)
    is_first = jnp.logical_and(z == 0, y == 0)
    ext[0:8, :] = jnp.where(is_first, 0.0, hist_inner[8:16, :].astype(F32))
    ext_c[0:8] = jnp.where(is_first, 0.0, hist_coeff[...].astype(F32))
    taps(0)
    block_state(0)
    own[...] = (
        states[0] * per_head(jnp.exp(ends[1] + ends[2])) + states[1] * per_head(jnp.exp(ends[2])) + states[2]
    ).astype(BF)

    slice_of = lambda v: pl.ds(pl.multiple_of(v * SLICE, SLICE), SLICE)
    st1_landed = to_all(lambda d: own.at[slice_of(at(y, d))], (st_row.at[y], st_row.at[seven]), along_y)
    event(1)
    st_row[y] = own[slice_of(y), :]

    def inside(b):
        rb = slice(b * BLOCK, (b + 1) * BLOCK)
        scores = dot(act[rb, INNER + STATE :], act[rb, INNER : INNER + STATE], NT)
        for j in range(HEADS // 2):
            lanes = slice(128 * j, 128 * (j + 1))
            parts = []
            for h in (2 * j, 2 * j + 1):
                gap = cum[rb, h : h + 1] - cum_t[h : h + 1, rb]
                within = jnp.exp(jnp.where(causal, gap, -1e30)) * (scores * step_t[h : h + 1, rb])
                parts.append(dot(within.astype(BF), act[rb, lanes], NN))
            local[rb, lanes] = jnp.where(low_lanes, parts[0], parts[1])

    def carried(b):
        rb = slice(b * BLOCK, (b + 1) * BLOCK)
        if b == 1:
            inner_state = states[0]
        else:
            inner_state = states[0] * per_head(jnp.exp(ends[1])) + states[1]
        local[rb, :] += dot(act[rb, INNER + STATE :], inner_state.astype(BF), NN) * per_head(jnp.exp(cum[rb, :]))

    ld_landed()
    row_logs = ld_row[:, 0, :]
    ld_total[...] = jnp.broadcast_to(jnp.sum(row_logs, axis=0, keepdims=True), (8, 128))
    ld2_landed = to_all(lambda d: ld_total, (ld_rows.at[z], ld_rows.at[seven]), along_z)
    ld_rows[z] = ld_total[...]
    row_decay = per_head(jnp.exp(row_logs))

    inside(0)
    inside(1)
    inside(2)
    carried(1)
    carried(2)
    st1_landed()
    run = jnp.zeros((SLICE, INNER), F32)
    for k in range(N):
        pre[k] = run
        run = run * row_decay[k : k + 1, :] + st_row[k].astype(F32)
    st_total[...] = run.astype(BF)
    st2_landed = to_all(lambda d: st_total, (st_rows.at[z], st_rows.at[seven]), along_z)
    st_rows[z] = st_total[...]
    event(2)
    ld2_landed()
    rows_decay = per_head(jnp.exp(ld_rows[:, 0, :]))
    st2_landed()
    run = jnp.zeros((SLICE, INNER), F32)
    for k in range(N):
        run = jnp.where(k < z, run * rows_decay[k : k + 1, :] + st_rows[k].astype(F32), run)
    for k in range(N):
        st_back[k] = (pre[k] + run).astype(BF)
        if k < N - 1:
            run = run * row_decay[k : k + 1, :]
    st3_landed = to_all(
        lambda d: st_back.at[at(y, d)], (enter.at[slice_of(y)], enter.at[pl.ds(0, SLICE * (N - 1))]), along_y
    )
    enter[slice_of(y), :] = st_back[y]

    event(3)
    st3_landed()
    event(4)
    gate_copy.wait()
    start_log = jnp.zeros_like(ends[0])
    for b in range(NB):
        rb = slice(b * BLOCK, (b + 1) * BLOCK)
        outer = dot(act[rb, INNER + STATE :], enter[...], NN) * per_head(jnp.exp(cum[rb, :] + start_log))
        gated = (local[rb, :] + outer) * silu(gate[rb, :].astype(F32))
        mean = jnp.mean(gated * gated, axis=1, keepdims=True)
        mixed[rb, :] = (gated * lax.rsqrt(mean + EPS) * mixer_gain[...]).astype(BF)
        start_log = start_log + ends[b]

    top, bottom = pl.ds(0, HALF), pl.ds(HALF, HALF)

    def reduced(block, use, pumps):
        pair_sent, ring_sent = sender(rows.at[pl.ds(0, NX)]), sender(rows.at[pl.ds(0, 3)])
        pair_landed = [receiver() for _ in range(NX)]
        from_l, from_r, final = receiver(), receiver(), receiver()

        def both(i, dx):
            value = block(atx(dx))
            lower, upper = value[:, :COLS], value[:, COLS:]
            pair_out[use, i] = jnp.where(c == 0, upper, lower).astype(BF)
            go(pair_out.at[use, i], pair_in.at[use, i], partner, pair_sent, pair_landed[i])
            keep[i] = jnp.where(c == 0, lower, upper)

        def mine(i):
            landed(pair_landed[i], rows.at[0])
            return keep[i] + pair_in[use, i].astype(F32)

        both(0, 2)
        both(1, 1)
        pumps[0]()
        far[use] = mine(0).astype(BF)
        go(far.at[use, top], relay_l.at[use], right, ring_sent, from_l)
        go(far.at[use, bottom], relay_r.at[use], left, ring_sent, from_r)
        both(2, 3)
        value = mine(1)
        keep[1] = value
        near_r[use, HALF:, :] = value[HALF:].astype(BF)
        go(near_r.at[use, bottom], fin_l.at[use, bottom], right, ring_sent, final)
        both(3, 0)
        value = mine(2)
        keep[2] = value
        near_l[use, :HALF, :] = value[:HALF].astype(BF)
        go(near_l.at[use, top], fin_r.at[use, top], left, ring_sent, final)
        keep[3] = mine(3)
        landed(from_l, relay_l.at[use])
        near_r[use, :HALF, :] = (keep[1, :HALF, :] + relay_l[use].astype(F32)).astype(BF)
        go(near_r.at[use, top], fin_l.at[use, top], right, ring_sent, final)
        landed(from_r, relay_r.at[use])
        near_l[use, HALF:, :] = (keep[2, HALF:, :] + relay_r[use].astype(F32)).astype(BF)
        go(near_l.at[use, bottom], fin_r.at[use, bottom], left, ring_sent, final)
        pumps[1]()
        landed(final, rows.at[pl.ds(0, 2)])
        return keep[3] + fin_l[use].astype(F32) + fin_r[use].astype(F32)

    def out_block(chip):
        return dot(mixed[...], out_w[:, pl.ds(pl.multiple_of(chip * 2 * COLS, 2 * COLS), 2 * COLS)], NN)

    out_copy.wait()
    projected = reduced(out_block, 0, (lambda: event(5), lambda: event(6)))
    residual_copy.wait()
    first[...] = (residual[...].astype(F32) + projected).astype(BF)
    rows[tp] = first[...]

    mine_tp, left_tp, right_tp, far_tp = tp, 2 * atx(3) + c, 2 * atx(1) + c, 2 * atx(2) + c
    rows_sent = sender(rows.at[seven])
    l_first, r_first, l_second, r_second, far_landed, across_landed = (receiver() for _ in range(6))
    go(first.at[top], rows.at[tp, top], right, rows_sent, l_first)
    go(first.at[bottom], rows.at[tp, bottom], left, rows_sent, r_first)
    go(first, rows.at[tp], partner, rows_sent, across_landed)
    go(first.at[bottom], rows.at[tp, bottom], right, rows_sent, l_second)
    go(first.at[top], rows.at[tp, top], left, rows_sent, r_second)
    event(7)
    gain_landed()
    squares = jnp.zeros((ROWS, 1), F32)

    def raise_rows(source, squares, new=False):
        wide = rows[source].astype(F32)
        squares = squares + jnp.sum(wide * wide, axis=1, keepdims=True)
        scaled = (wide * gain_all[source][0:1, :]).astype(BF)
        weights = up_all[source].reshape(COLS, FF)
        product = dot(scaled, weights, NN)
        acc[...] = product if new else acc[...] + product
        return squares

    landed(l_first, relay_l.at[0])
    go(rows.at[left_tp, top], rows.at[left_tp, top], right, rows_sent, far_landed)
    landed(r_first, relay_l.at[0])
    go(rows.at[right_tp, bottom], rows.at[right_tp, bottom], left, rows_sent, far_landed)
    landed(l_second, relay_l.at[0])
    go(rows.at[left_tp], rows.at[left_tp], partner, rows_sent, across_landed)
    landed(r_second, relay_l.at[0])
    go(rows.at[right_tp], rows.at[right_tp], partner, rows_sent, across_landed)
    event(8)
    landed(far_landed, rows.at[0])
    go(rows.at[far_tp], rows.at[far_tp], partner, rows_sent, across_landed)
    landed(across_landed, rows.at[pl.ds(0, NX)])
    event(9)
    for batch in range(2):
        pieces_landed(0, 1, 4, batch)
    for k in (0, N - 1, 1):
        squares = raise_rows(at(z, k), squares, k == 0)
    event(10)
    for batch, sources in ((2, (N - 2, 2)), (3, (N - 3, 3)), (4, (4,))):
        pieces_landed(0, 1, 4, batch)
        for k in sources:
            squares = raise_rows(at(z, k), squares)
    scale = lax.rsqrt(squares * (1.0 / D) + EPS)
    active[...] = jnp.square(jnp.maximum(acc[...] * scale, 0.0)).astype(BF)

    def down_block(chip):
        return dot(active[...], down_all[pl.ds(2 * chip, 2)].reshape(2 * COLS, FF), NT)

    for batch in range(5):
        pieces_landed(1, 1, 4, batch)
    nothing = lambda: None
    lowered = reduced(down_block, 1, (nothing, nothing))
    result[...] = (first[...].astype(F32) + lowered).astype(BF)
    for sent, total in pending:
        remote(total, total, partner, sent, recv.at[0]).wait_send()


def shards(
    inner_pre, coeff_pre, gate_pre, step_raw, step_bias, decay_log, conv_inner, conv_coeff, mixer_gain,
    out_weight, residual, mlp_gain, up_weight, down_weight,
):
    vm = pltpu.VMEM
    dma = pltpu.SemaphoreType.DMA
    in_vmem = pl.BlockSpec(memory_space=pltpu.VMEM)
    specs = [in_vmem] * 14
    for i in (0, 1, 2, 9, 10, 12, 13):
        specs[i] = pl.BlockSpec(memory_space=pl.ANY)
    scratch = [
        vm((ROWS, INNER), BF), vm((ROWS, 2, STATE), BF), vm((ROWS, INNER), BF), vm((ROWS, COLS), BF),
        vm((PIECE, FF), BF), vm((PIECE, FF), BF),
        vm((EDGE, INNER), BF), vm((8, 2, STATE), BF), vm((ROWS + 8, INNER), F32), vm((ROWS + 8, 2, STATE), F32), vm((ROWS, INNER + COLS), BF),
        vm((ROWS, HEADS), F32), vm((HEADS, ROWS), F32), vm((ROWS, HEADS), F32), vm((HEADS, ROWS), F32),
        vm((ROWS, INNER), F32), vm((NB, STATE, INNER), F32), vm((STATE, INNER), BF), vm((STATE, INNER), BF),
        vm((8, 128), F32), vm((N, 8, 128), F32), vm((8, 128), F32), vm((N, 8, 128), F32),
        vm((N, SLICE, INNER), F32), vm((N, SLICE, INNER), BF), vm((SLICE, INNER), BF), vm((N, SLICE, INNER), BF),
        vm((N, SLICE, INNER), BF),
        vm((ROWS, INNER), BF), vm((INNER, D), BF), vm((N, N, PIECE, FF), BF), vm((N, N, PIECE, FF), BF),
        vm((8, COLS), F32), vm((N, 8, COLS), F32),
        vm((2, NX, ROWS, COLS), BF), vm((2, NX, ROWS, COLS), BF), vm((2, ROWS, COLS), BF),
        vm((2, HALF, COLS), BF), vm((2, HALF, COLS), BF), vm((2, ROWS, COLS), BF), vm((2, ROWS, COLS), BF),
        vm((2, ROWS, COLS), BF), vm((2, ROWS, COLS), BF), vm((NX, ROWS, COLS), F32),
        vm((N, ROWS, COLS), BF), vm((ROWS, COLS), BF), vm((ROWS, FF), F32), vm((ROWS, FF), BF),
        dma((17,)), dma((76,)), dma((7,)),
    ]
    return pl.pallas_call(
        kernel,
        out_shape=jax.ShapeDtypeStruct((ROWS, COLS), BF),
        in_specs=specs,
        out_specs=in_vmem,
        scratch_shapes=scratch,
        compiler_params=pltpu.CompilerParams(
            collective_id=0, has_side_effects=True, vmem_limit_bytes=60 * 1024 * 1024
        ),
        name="layer",
    )(
        inner_pre, coeff_pre, gate_pre, step_raw.T, step_bias[None], decay_log[None], conv_inner,
        conv_coeff, mixer_gain[None], out_weight, residual, mlp_gain[None], up_weight, down_weight.T,
    )


def solution(mesh):
    split = Mesh(mesh.devices.reshape(N, N, NX, 2), ("z", "y", "x", "c"))
    sp, tp = ("z", "y"), ("x", "c")
    return jax.shard_map(
        shards,
        mesh=split,
        in_specs=(
            P(sp, tp), P(sp, None, tp), P(sp, tp), P(sp, tp), P(tp), P(tp), P(None, tp), P(None, None, tp), P(tp),
            P(tp, None), P(sp, tp), P(tp), P(sp, tp), P(tp, sp),
        ),
        out_specs=P(sp, tp),
        check_vma=False,
    )
```

time: 106 us -> 84 us (0.79)
  Pallas kernels: 99.7 us -> 82.2 us
  local copies, waits for them, and re-layouts: 5.98 us -> 1.62 us
    pallas_call x1, Pallas kernels: 99.7 us -> 82.2 us  [shards(): pl.pallas_call(kernel, out_shape=jax.ShapeDtypeStruct((ROWS, COLS), BF),...]
    unnamed x4 -> x1, local copies, waits for them, and re-layouts: 5.98 us -> 1.62 us
where the time goes in v2:
time: 84 us; the launch traced here: 83.8 us
  Pallas kernels  82.2 us (98%)
  local copies, waits for them, and re-layouts  1.62 us (2%)
    pallas_call x1, Pallas kernels, shards(): pl.pallas_call(kernel, out_shape=jax.ShapeDtypeStruct((ROWS, COLS), BF),...  82.2 us

profile of v2, /device:TPU:1, one launch (start us, length us, event | category | flops | bytes accessed | tf_op | source)
XLA Modules:
  0.0 83.8 jit_solution(11873694259751816183)
XLA Ops:
  0.0 82.2 %layer.1 = bf16[384,256]{1,0:T(8,128)(2,1)} custom-call(bf16[384,512]{1,0:T(8,128)(2,1)} %inner_hbm.1, bf16[384,2,128]{2,1,0:T(2,128)(2,1)} %coeff_hbm.1, bf16[384,512]{1,0:T(8,128)(2,1)} %gate_hbm.1, bf16[8,384]{1,0:T(8,128)(2,1)} %bitcast.7, f32[1,8]{1,0:T(1,128)} %bitcast.10, f32[1,8]{1,0:T(1,128)} %bitcast.11, bf16[4,512]{1,0:T(4,128)(2,1)} %taps_inner.1, ...), custom_call_target="tpu_custom_call" | custom-call | tf_op jit(solution)/shard_map/layer/pallas_call | solution.py:493
  82.2 1.6 %copy.16 = bf16[384,256]{1,0:T(8,128)(2,1)} copy(bf16[384,256]{1,0:T(8,128)(2,1)} %layer.1) | data formatting | bytes 393216

commit v3 on v2

--- a/solution.py
+++ b/solution.py
@@ -49,15 +49,14 @@
 
 
 def kernel(
-    inner_hbm, coeff_hbm, gate_hbm, step_raw, step_bias, decay_log, taps_inner, taps_coeff, mixer_gain,
-    out_hbm, residual_hbm, mlp_gain, up_hbm, down_hbm, result,
-    inner, coeff, gate, residual, up, down,
+    inner_hbm, coeff_hbm, gate_hbm, step_raw_hbm, step_bias_hbm, decay_log_hbm, taps_inner_hbm, taps_coeff_hbm,
+    mixer_gain_hbm, out_hbm, residual_hbm, mlp_gain_hbm, up_hbm, down_hbm, result,
+    inner, coeff, gate, residual, up, down, step_raw, step_bias, decay_log, taps_inner, taps_coeff, mixer_gain,
+    mlp_gain,
     hist_inner, hist_coeff, ext, ext_c, act, cum, cum_t, step, step_t, local, states, own, enter,
     ld_own, ld_row, ld_total, ld_rows, pre, st_row, st_total, st_rows, st_back,
     mixed, out_w, up_all, down_all, gain_own, gain_all,
-    pair_out, pair_in, far, relay_l, relay_r, near_l, near_r, fin_l, fin_r, keep,
-    rows, first, acc, active,
-    send, recv, local_sem,
+    rows, first, acc, active, send, recv, local_sem, *reductions,
 ):
     z, y, x, c = (lax.axis_index(a) for a in ("z", "y", "x", "c"))
     tp = 2 * x + c
@@ -80,14 +79,16 @@
         pltpu.make_async_copy(there, here, local_sem.at[i])
         for i, (there, here) in enumerate(
             (
-                (up_hbm, up), (down_hbm, down), (inner_hbm, inner), (coeff_hbm, coeff), (gate_hbm, gate),
-                (residual_hbm, residual), (out_hbm, out_w),
+                (step_raw_hbm, step_raw), (step_bias_hbm, step_bias), (decay_log_hbm, decay_log),
+                (mlp_gain_hbm, mlp_gain), (taps_inner_hbm, taps_inner), (taps_coeff_hbm, taps_coeff),
+                (up_hbm, up), (down_hbm, down), (inner_hbm, inner), (coeff_hbm, coeff),
+                (mixer_gain_hbm, mixer_gain), (gate_hbm, gate), (residual_hbm, residual), (out_hbm, out_w),
             )
         )
     ]
     for copy in fetched:
         copy.start()
-    up_copy, down_copy, inner_copy, coeff_copy, gate_copy, residual_copy, out_copy = fetched
+    up_copy, down_copy, inner_copy, coeff_copy, mixer_gain_copy, gate_copy, residual_copy, out_copy = fetched[6:]
 
     used = [0, 0]
     pending = []
@@ -122,6 +123,8 @@
 
     on_heads = lax.broadcasted_iota(jnp.int32, (HEADS, HEADS), 0) == lax.broadcasted_iota(jnp.int32, (HEADS, HEADS), 1)
     column = lambda v: jnp.sum(jnp.where(on_heads, jnp.broadcast_to(v, (HEADS, HEADS)), 0.0), axis=1, keepdims=True)
+    for copy in fetched[:6]:
+        copy.wait()
     bias = column(step_bias[...])
     rate = jnp.exp(column(decay_log[...]))
     ends = []
@@ -173,21 +176,23 @@
     def forward(weight, stage, way, hop, batch=0, offset=0):
         back = (N - (hop - 1)) % N if way == 0 else hop - 1
         to = 1 if way == 0 else N - 1
-        a, b = (z, y) if weight == 0 else (y, z)
-        a_axis, b_axis = ("z", "y") if weight == 0 else ("y", "z")
+        whole, piece = (up_all, up) if weight == 0 else (down_all, down)
         arrived = weights_landed[weight][stage][hop - 1]
-        if stage == 0:
-            ia, ib, where = at(a, back), b, {a_axis: at(a, to)}
-        else:
-            ia, ib, where = at(a, offset), at(b, back), {b_axis: at(b, to)}
-            arrived = arrived[batch]
-        ref = up_all.at[ia, ib] if weight == 0 else down_all.at[ib, ia]
-        source = ref
-        if hop == 1 and offset == 0:
-            source = up if weight == 0 else down
-        if hop == 4:
-            ref = source = ref.at[pl.ds(16 * way, 16)]
-        go(source, ref, where, weights_sent[weight][stage], arrived)
+        arrived = arrived if stage == 0 else arrived[batch]
+        columns = slice(None) if hop < 4 else pl.ds(way * (FF // 2), FF // 2)
+        for order in range(2):
+            part = pl.ds(order * (PIECE // 2), PIECE // 2)
+            a, b = (z, y) if order == 0 else (y, z)
+            if stage == 0:
+                ia, ib = at(a, back), b
+            else:
+                ia, ib = at(a, offset), at(b, back)
+            on_z = (stage == 0) == (order == 0)
+            where = {"z": at(z, to)} if on_z else {"y": at(y, to)}
+            iz, iy = (ia, ib) if order == 0 else (ib, ia)
+            ref = whole.at[iz, iy, part, columns]
+            source = piece.at[part] if hop == 1 and offset == 0 else ref
+            go(source, ref, where, weights_sent[weight][stage], arrived)
 
     def pieces_landed(weight, stage, hop, batch=0):
         count = len(OFFSETS[batch]) * (1 if hop == 4 else 2)
@@ -198,34 +203,26 @@
             arrived = arrived[batch]
         landed(arrived, (up_all if weight == 0 else down_all).at[0, pl.ds(0, count)])
 
-    def along(hop):
-        for w in range(2):
-            if hop > 1:
-                pieces_landed(w, 0, hop - 1)
-            if hop < 5:
-                forward(w, 0, 0, hop)
-                forward(w, 0, 1, hop)
-
-    def across_to(hop, batch):
-        for w in range(2):
-            if hop > 1:
-                pieces_landed(w, 1, hop - 1, batch)
-            for offset in OFFSETS[batch]:
-                forward(w, 1, 0, hop, batch, offset)
-                forward(w, 1, 1, hop, batch, offset)
-
-    def event(k):
-        if k < 5:
-            along(k + 1)
-        for hop, batch in EVENTS[k]:
-            across_to(hop, batch)
-
-    EVENTS = (
-        ((1, 0),),
-        ((1, 1),),
-        ((1, 2), (2, 0)),
-        ((1, 3), (2, 1)),
-        ((1, 4), (2, 2), (3, 0)),
+    def along(weight, hop):
+        if hop > 1:
+            pieces_landed(weight, 0, hop - 1)
+        if hop < 5:
+            forward(weight, 0, 0, hop)
+            forward(weight, 0, 1, hop)
+
+    def across_to(weight, hop, batch):
+        if hop > 1:
+            pieces_landed(weight, 1, hop - 1, batch)
+        for offset in OFFSETS[batch]:
+            forward(weight, 1, 0, hop, batch, offset)
+            forward(weight, 1, 1, hop, batch, offset)
+
+    UP = (
+        (1, (1, 0)),
+        (2, (1, 1)),
+        (3, (1, 2), (2, 0)),
+        (4, (1, 3), (2, 1)),
+        (5, (1, 4), (2, 2), (3, 0)),
         ((2, 3), (3, 1)),
         ((2, 4), (3, 2), (4, 0)),
         ((3, 3), (4, 1)),
@@ -233,7 +230,37 @@
         ((4, 3),),
         ((4, 4),),
     )
+    DOWN = (
+        (1, (1, 0)),
+        (2, (1, 1)),
+        (3, (2, 0)),
+        ((1, 2), 4, (2, 1)),
+        ((1, 3), (3, 0)),
+        (5, (1, 4), (2, 2)),
+        ((2, 3), (3, 1)),
+        ((2, 4), (3, 2), (4, 0)),
+        ((3, 3),),
+        ((3, 4),),
+        ((4, 1), (4, 2)),
+        ((4, 3),),
+        ((4, 4),),
+    )
+
+    def rounds(weight, items):
+        for item in items:
+            if isinstance(item, int):
+                along(weight, item)
+            else:
+                across_to(weight, *item)
+
+    def event(k):
+        rounds(0, UP[k])
+
+    def fill(k):
+        rounds(1, DOWN[k])
+
     event(0)
+    fill(0)
     up_all[z, y] = up[...]
     down_all[z, y] = down[...]
 
@@ -280,6 +307,7 @@
     slice_of = lambda v: pl.ds(pl.multiple_of(v * SLICE, SLICE), SLICE)
     st1_landed = to_all(lambda d: own.at[slice_of(at(y, d))], (st_row.at[y], st_row.at[seven]), along_y)
     event(1)
+    fill(1)
     st_row[y] = own[slice_of(y), :]
 
     def inside(b):
@@ -323,6 +351,7 @@
     st2_landed = to_all(lambda d: st_total, (st_rows.at[z], st_rows.at[seven]), along_z)
     st_rows[z] = st_total[...]
     event(2)
+    fill(2)
     ld2_landed()
     rows_decay = per_head(jnp.exp(ld_rows[:, 0, :]))
     st2_landed()
@@ -339,8 +368,11 @@
     enter[slice_of(y), :] = st_back[y]
 
     event(3)
+    fill(3)
     st3_landed()
     event(4)
+    fill(4)
+    mixer_gain_copy.wait()
     gate_copy.wait()
     start_log = jnp.zeros_like(ends[0])
     for b in range(NB):
@@ -353,54 +385,80 @@
 
     top, bottom = pl.ds(0, HALF), pl.ds(HALF, HALF)
 
-    def reduced(block, use, pumps):
-        pair_sent, ring_sent = sender(rows.at[pl.ds(0, NX)]), sender(rows.at[pl.ds(0, 3)])
-        pair_landed = [receiver() for _ in range(NX)]
-        from_l, from_r, final = receiver(), receiver(), receiver()
-
-        def both(i, dx):
-            value = block(atx(dx))
-            lower, upper = value[:, :COLS], value[:, COLS:]
-            pair_out[use, i] = jnp.where(c == 0, upper, lower).astype(BF)
-            go(pair_out.at[use, i], pair_in.at[use, i], partner, pair_sent, pair_landed[i])
-            keep[i] = jnp.where(c == 0, lower, upper)
-
-        def mine(i):
-            landed(pair_landed[i], rows.at[0])
-            return keep[i] + pair_in[use, i].astype(F32)
-
-        both(0, 2)
-        both(1, 1)
-        pumps[0]()
-        far[use] = mine(0).astype(BF)
-        go(far.at[use, top], relay_l.at[use], right, ring_sent, from_l)
-        go(far.at[use, bottom], relay_r.at[use], left, ring_sent, from_r)
-        both(2, 3)
-        value = mine(1)
-        keep[1] = value
-        near_r[use, HALF:, :] = value[HALF:].astype(BF)
-        go(near_r.at[use, bottom], fin_l.at[use, bottom], right, ring_sent, final)
-        both(3, 0)
-        value = mine(2)
-        keep[2] = value
-        near_l[use, :HALF, :] = value[:HALF].astype(BF)
-        go(near_l.at[use, top], fin_r.at[use, top], left, ring_sent, final)
-        keep[3] = mine(3)
-        landed(from_l, relay_l.at[use])
-        near_r[use, :HALF, :] = (keep[1, :HALF, :] + relay_l[use].astype(F32)).astype(BF)
-        go(near_r.at[use, top], fin_l.at[use, top], right, ring_sent, final)
-        landed(from_r, relay_r.at[use])
-        near_l[use, HALF:, :] = (keep[2, HALF:, :] + relay_r[use].astype(F32)).astype(BF)
-        go(near_l.at[use, bottom], fin_r.at[use, bottom], left, ring_sent, final)
-        pumps[1]()
-        landed(final, rows.at[pl.ds(0, 2)])
-        return keep[3] + fin_l[use].astype(F32) + fin_r[use].astype(F32)
+    class Reduction:
+        def __init__(self, block, refs):
+            self.block = block
+            self.pair_out, self.pair_in, self.far, self.relay, self.near, self.fin, self.keep = refs
+            self.pair_sent, self.ring_sent = sender(self.pair_in), sender(self.pair_in.at[pl.ds(0, 3)])
+            self.pair_landed = [receiver() for _ in range(NX)]
+            self.from_l, self.from_r, self.final = receiver(), receiver(), receiver()
+
+        def both(self, *members):
+            value = self.block(*[atx((2, 1, 3, 0)[i]) for i in members])
+            width = value.shape[1] // len(members)
+            for n, i in enumerate(members):
+                self.share(i, value[:, n * width : (n + 1) * width])
+
+        def share(self, i, value):
+            width = value.shape[1] // 2
+            lower, upper = value[:, :width], value[:, width:]
+            self.pair_out[i] = jnp.where(c == 0, upper, lower).astype(BF)
+            go(self.pair_out.at[i], self.pair_in.at[i], partner, self.pair_sent, self.pair_landed[i])
+            self.keep[i] = jnp.where(c == 0, lower, upper)
+
+        def mine(self, i):
+            landed(self.pair_landed[i], self.pair_in.at[i])
+            return self.keep[i] + self.pair_in[i].astype(F32)
+
+        def send_far(self):
+            self.far[...] = self.mine(0).astype(BF)
+            go(self.far.at[top], self.relay.at[0], right, self.ring_sent, self.from_l)
+            go(self.far.at[bottom], self.relay.at[1], left, self.ring_sent, self.from_r)
+
+        def send_right(self):
+            self.keep[1] = value = self.mine(1)
+            self.near[0, HALF:, :] = value[HALF:].astype(BF)
+            go(self.near.at[0, bottom], self.fin.at[0, bottom], right, self.ring_sent, self.final)
+
+        def send_left(self):
+            self.keep[2] = value = self.mine(2)
+            self.near[1, :HALF, :] = value[:HALF].astype(BF)
+            go(self.near.at[1, top], self.fin.at[1, top], left, self.ring_sent, self.final)
+
+        def own(self):
+            self.keep[3] = self.mine(3)
+
+        def pass_on(self):
+            landed(self.from_l, self.relay.at[0])
+            self.near[0, :HALF, :] = (self.keep[1, :HALF, :] + self.relay[0].astype(F32)).astype(BF)
+            go(self.near.at[0, top], self.fin.at[0, top], right, self.ring_sent, self.final)
+            landed(self.from_r, self.relay.at[1])
+            self.near[1, HALF:, :] = (self.keep[2, HALF:, :] + self.relay[1].astype(F32)).astype(BF)
+            go(self.near.at[1, bottom], self.fin.at[1, bottom], left, self.ring_sent, self.final)
+
+        def total(self):
+            landed(self.final, self.fin)
+            return self.keep[3] + self.fin[0].astype(F32) + self.fin[1].astype(F32)
 
     def out_block(chip):
         return dot(mixed[...], out_w[:, pl.ds(pl.multiple_of(chip * 2 * COLS, 2 * COLS), 2 * COLS)], NN)
 
     out_copy.wait()
-    projected = reduced(out_block, 0, (lambda: event(5), lambda: event(6)))
+    mixer_sum = Reduction(out_block, reductions[0:7])
+    mixer_sum.both(0)
+    mixer_sum.both(1)
+    mixer_sum.send_far()
+    mixer_sum.both(2)
+    mixer_sum.send_right()
+    mixer_sum.both(3)
+    mixer_sum.send_left()
+    mixer_sum.own()
+    event(5)
+    fill(5)
+    mixer_sum.pass_on()
+    event(6)
+    fill(6)
+    projected = mixer_sum.total()
     residual_copy.wait()
     first[...] = (residual[...].astype(F32) + projected).astype(BF)
     rows[tp] = first[...]
@@ -414,6 +472,7 @@
     go(first.at[bottom], rows.at[tp, bottom], right, rows_sent, l_second)
     go(first.at[top], rows.at[tp, top], left, rows_sent, r_second)
     event(7)
+    fill(7)
     gain_landed()
     squares = jnp.zeros((ROWS, 1), F32)
 
@@ -426,38 +485,67 @@
         acc[...] = product if new else acc[...] + product
         return squares
 
-    landed(l_first, relay_l.at[0])
+    half_rows = rows.at[0, top]
+    landed(l_first, half_rows)
     go(rows.at[left_tp, top], rows.at[left_tp, top], right, rows_sent, far_landed)
-    landed(r_first, relay_l.at[0])
+    landed(r_first, half_rows)
     go(rows.at[right_tp, bottom], rows.at[right_tp, bottom], left, rows_sent, far_landed)
-    landed(l_second, relay_l.at[0])
+    event(8)
+    fill(8)
+    landed(l_second, half_rows)
     go(rows.at[left_tp], rows.at[left_tp], partner, rows_sent, across_landed)
-    landed(r_second, relay_l.at[0])
+    landed(r_second, half_rows)
     go(rows.at[right_tp], rows.at[right_tp], partner, rows_sent, across_landed)
-    event(8)
+    event(9)
+    fill(9)
     landed(far_landed, rows.at[0])
     go(rows.at[far_tp], rows.at[far_tp], partner, rows_sent, across_landed)
+    event(10)
+    fill(10)
     landed(across_landed, rows.at[pl.ds(0, NX)])
-    event(9)
-    for batch in range(2):
+    fill(11)
+    for batch in range(5):
         pieces_landed(0, 1, 4, batch)
-    for k in (0, N - 1, 1):
-        squares = raise_rows(at(z, k), squares, k == 0)
-    event(10)
-    for batch, sources in ((2, (N - 2, 2)), (3, (N - 3, 3)), (4, (4,))):
-        pieces_landed(0, 1, 4, batch)
-        for k in sources:
-            squares = raise_rows(at(z, k), squares)
+    fill(12)
+    for k in range(N):
+        squares = raise_rows(k, squares, k == 0)
     scale = lax.rsqrt(squares * (1.0 / D) + EPS)
     active[...] = jnp.square(jnp.maximum(acc[...] * scale, 0.0)).astype(BF)
 
-    def down_block(chip):
-        return dot(active[...], down_all[pl.ds(2 * chip, 2)].reshape(2 * COLS, FF), NT)
-
-    for batch in range(5):
+    def down_block(half):
+        def block(*chips):
+            pieces = [
+                down_all[2 * chip + j, at(y, (N - 1 + 4 * half + p) % N)]
+                for chip in chips
+                for j in range(2)
+                for p in range(4)
+            ]
+            return dot(active[...], jnp.concatenate(pieces, axis=0), NT)
+
+        return block
+
+    early, late = Reduction(down_block(0), reductions[7:14]), Reduction(down_block(1), reductions[14:21])
+    for batch in range(3):
         pieces_landed(1, 1, 4, batch)
-    nothing = lambda: None
-    lowered = reduced(down_block, 1, (nothing, nothing))
+    early.both(0, 1)
+    early.both(2, 3)
+    early.send_far()
+    early.send_right()
+    early.send_left()
+    for batch in range(3, 5):
+        pieces_landed(1, 1, 4, batch)
+    late.both(0, 1)
+    early.own()
+    late.both(2, 3)
+    late.send_far()
+    early.pass_on()
+    late.send_right()
+    late.send_left()
+    late.own()
+    late.pass_on()
+    turned = early.total()
+    turned = jnp.concatenate([turned, late.total()], axis=1)
+    lowered = pltpu.roll(turned, at(y, N - 1) * PIECE, 1)
     result[...] = (first[...].astype(F32) + lowered).astype(BF)
     for sent, total in pending:
         remote(total, total, partner, sent, recv.at[0]).wait_send()
@@ -469,13 +557,10 @@
 ):
     vm = pltpu.VMEM
     dma = pltpu.SemaphoreType.DMA
-    in_vmem = pl.BlockSpec(memory_space=pltpu.VMEM)
-    specs = [in_vmem] * 14
-    for i in (0, 1, 2, 9, 10, 12, 13):
-        specs[i] = pl.BlockSpec(memory_space=pl.ANY)
     scratch = [
         vm((ROWS, INNER), BF), vm((ROWS, 2, STATE), BF), vm((ROWS, INNER), BF), vm((ROWS, COLS), BF),
-        vm((PIECE, FF), BF), vm((PIECE, FF), BF),
+        vm((PIECE, FF), BF), vm((PIECE, FF), BF), vm((HEADS, ROWS), BF), vm((1, HEADS), F32), vm((1, HEADS), F32),
+        vm((4, INNER), BF), vm((4, 2, STATE), BF), vm((1, INNER), F32), vm((1, COLS), F32),
         vm((EDGE, INNER), BF), vm((8, 2, STATE), BF), vm((ROWS + 8, INNER), F32), vm((ROWS + 8, 2, STATE), F32), vm((ROWS, INNER + COLS), BF),
         vm((ROWS, HEADS), F32), vm((HEADS, ROWS), F32), vm((ROWS, HEADS), F32), vm((HEADS, ROWS), F32),
         vm((ROWS, INNER), F32), vm((NB, STATE, INNER), F32), vm((STATE, INNER), BF), vm((STATE, INNER), BF),
@@ -484,17 +569,19 @@
         vm((N, SLICE, INNER), BF),
         vm((ROWS, INNER), BF), vm((INNER, D), BF), vm((N, N, PIECE, FF), BF), vm((N, N, PIECE, FF), BF),
         vm((8, COLS), F32), vm((N, 8, COLS), F32),
-        vm((2, NX, ROWS, COLS), BF), vm((2, NX, ROWS, COLS), BF), vm((2, ROWS, COLS), BF),
-        vm((2, HALF, COLS), BF), vm((2, HALF, COLS), BF), vm((2, ROWS, COLS), BF), vm((2, ROWS, COLS), BF),
-        vm((2, ROWS, COLS), BF), vm((2, ROWS, COLS), BF), vm((NX, ROWS, COLS), F32),
         vm((N, ROWS, COLS), BF), vm((ROWS, COLS), BF), vm((ROWS, FF), F32), vm((ROWS, FF), BF),
-        dma((17,)), dma((76,)), dma((7,)),
+        dma((19,)), dma((83,)), dma((14,)),
     ]
+    for width in (COLS, COLS // 2, COLS // 2):
+        scratch += [
+            vm((NX, ROWS, width), BF), vm((NX, ROWS, width), BF), vm((ROWS, width), BF), vm((2, HALF, width), BF),
+            vm((2, ROWS, width), BF), vm((2, ROWS, width), BF), vm((NX, ROWS, width), F32),
+        ]
     return pl.pallas_call(
         kernel,
-        out_shape=jax.ShapeDtypeStruct((ROWS, COLS), BF),
-        in_specs=specs,
-        out_specs=in_vmem,
+        out_shape=pltpu.VMEM((ROWS, COLS), BF),
+        in_specs=[pl.BlockSpec(memory_space=pltpu.HBM)] * 14,
+        out_specs=pl.BlockSpec(memory_space=pltpu.VMEM),
         scratch_shapes=scratch,
         compiler_params=pltpu.CompilerParams(
             collective_id=0, has_side_effects=True, vmem_limit_bytes=60 * 1024 * 1024

time: 84 us -> 80.7 us (0.961)
  Pallas kernels: 82.2 us -> 79.9 us
  local copies, waits for them, and re-layouts: 1.62 us -> 0.68 us
    pallas_call x1, Pallas kernels: 82.2 us -> 79.9 us  [shards(): pl.pallas_call(kernel, out_shape=pltpu.VMEM((ROWS, COLS), BF), in_specs=[...]
    unnamed x1, local copies, waits for them, and re-layouts: 1.62 us -> 0.68 us
where the time goes in v3:
time: 80.7 us; the launch traced here: 80.6 us
  Pallas kernels  79.9 us (99%)
    pallas_call x1, Pallas kernels, shards(): pl.pallas_call(kernel, out_shape=pltpu.VMEM((ROWS, COLS), BF), in_specs=[...  79.9 us

profile of v3, /device:TPU:1, one launch (start us, length us, event | category | flops | bytes accessed | tf_op | source)
XLA Modules:
  0.0 80.6 jit_solution(2230720996440966442)
XLA Ops:
  0.0 79.9 %layer.1 = bf16[384,256]{1,0:T(8,128)(2,1)S(1)} custom-call(bf16[384,512]{1,0:T(8,128)(2,1)} %inner_hbm.1, bf16[384,2,128]{2,1,0:T(2,128)(2,1)} %coeff_hbm.1, bf16[384,512]{1,0:T(8,128)(2,1)} %gate_hbm.1, bf16[8,384]{1,0:T(8,128)(2,1)} %bitcast.7, f32[1,8]{1,0:T(1,128)} %bitcast.10, f32[1,8]{1,0:T(1,128)} %bitcast.11, bf16[4,512]{1,0:T(4,128)(2,1)} %taps_inner_hbm.1, ...), custom_call_target="tpu_custom_call" | custom-call | tf_op jit(solution)/shard_map/layer/pallas_call | solution.py:580
  79.9 0.7 copy.16

commit v4 on v3

--- a/solution.py
+++ b/solution.py
@@ -141,7 +141,7 @@
         ends.append(cum_b[BLOCK - 1 : BLOCK, :])
     total = ends[0] + ends[1] + ends[2]
     ld_own[...] = jnp.zeros_like(ld_own)
-    ld_own[:, 0:HEADS] = jnp.broadcast_to(total, (8, HEADS))
+    ld_own[:, 0:HEADS] = total
     gain_own[...] = jnp.broadcast_to(mlp_gain[...], gain_own.shape)
 
     pl.semaphore_wait(barrier, len(greeted))
@@ -238,9 +238,9 @@
         ((1, 3), (3, 0)),
         (5, (1, 4), (2, 2)),
         ((2, 3), (3, 1)),
-        ((2, 4), (3, 2), (4, 0)),
-        ((3, 3),),
-        ((3, 4),),
+        ((2, 4),),
+        ((3, 2), (3, 3)),
+        ((3, 4), (4, 0)),
         ((4, 1), (4, 2)),
         ((4, 3),),
         ((4, 4),),
@@ -267,21 +267,24 @@
     ext[8 : 8 + ROWS, :] = inner[...].astype(F32)
     ext_c[8 : 8 + ROWS] = coeff[...].astype(F32)
 
-    def taps(b):
+    ext[0:8, :] = jnp.zeros((8, INNER), F32)
+    ext_c[0:8] = jnp.zeros((8, 2, STATE), F32)
+
+    def taps(b, count=BLOCK):
         for j in range(4):
             if j < 2:
                 lanes = slice(COLS * j, COLS * (j + 1))
                 weights = taps_inner[:, lanes].astype(F32)
-                shifted = lambda k: ext[pl.ds(b * BLOCK + 5 + k, BLOCK), lanes]
+                shifted = lambda k: ext[pl.ds(b * BLOCK + 5 + k, count), lanes]
                 target = lanes
             else:
                 weights = taps_coeff[...].astype(F32)[:, j - 2, :]
-                shifted = lambda k: ext_c[pl.ds(b * BLOCK + 5 + k, BLOCK), j - 2, :]
+                shifted = lambda k: ext_c[pl.ds(b * BLOCK + 5 + k, count), j - 2, :]
                 target = slice(INNER + STATE * (j - 2), INNER + STATE * (j - 1))
             total_taps = shifted(0) * weights[0:1]
             for k in range(1, 4):
                 total_taps = total_taps + shifted(k) * weights[k : k + 1]
-            act[b * BLOCK : (b + 1) * BLOCK, target] = silu(total_taps).astype(BF)
+            act[b * BLOCK : b * BLOCK + count, target] = silu(total_taps).astype(BF)
 
     def block_state(b):
         rb = slice(b * BLOCK, (b + 1) * BLOCK)
@@ -293,12 +296,13 @@
     taps(2)
     block_state(1)
     block_state(2)
+    taps(0)
     landed(inner_tail, hist_inner)
     landed(coeff_tail, hist_coeff)
     is_first = jnp.logical_and(z == 0, y == 0)
     ext[0:8, :] = jnp.where(is_first, 0.0, hist_inner[8:16, :].astype(F32))
     ext_c[0:8] = jnp.where(is_first, 0.0, hist_coeff[...].astype(F32))
-    taps(0)
+    taps(0, EDGE)
     block_state(0)
     own[...] = (
         states[0] * per_head(jnp.exp(ends[1] + ends[2])) + states[1] * per_head(jnp.exp(ends[2])) + states[2]
@@ -332,7 +336,7 @@
 
     ld_landed()
     row_logs = ld_row[:, 0, :]
-    ld_total[...] = jnp.broadcast_to(jnp.sum(row_logs, axis=0, keepdims=True), (8, 128))
+    ld_total[...] = jnp.sum(row_logs, axis=0, keepdims=True)
     ld2_landed = to_all(lambda d: ld_total, (ld_rows.at[z], ld_rows.at[seven]), along_z)
     ld_rows[z] = ld_total[...]
     row_decay = per_head(jnp.exp(row_logs))
@@ -497,18 +501,19 @@
     landed(r_second, half_rows)
     go(rows.at[right_tp], rows.at[right_tp], partner, rows_sent, across_landed)
     event(9)
-    fill(9)
     landed(far_landed, rows.at[0])
     go(rows.at[far_tp], rows.at[far_tp], partner, rows_sent, across_landed)
     event(10)
+    fill(9)
     fill(10)
     landed(across_landed, rows.at[pl.ds(0, NX)])
     fill(11)
     for batch in range(5):
         pieces_landed(0, 1, 4, batch)
-    fill(12)
     for k in range(N):
         squares = raise_rows(k, squares, k == 0)
+        if k == 2:
+            fill(12)
     scale = lax.rsqrt(squares * (1.0 / D) + EPS)
     active[...] = jnp.square(jnp.maximum(acc[...] * scale, 0.0)).astype(BF)
 
@@ -564,7 +569,7 @@
         vm((EDGE, INNER), BF), vm((8, 2, STATE), BF), vm((ROWS + 8, INNER), F32), vm((ROWS + 8, 2, STATE), F32), vm((ROWS, INNER + COLS), BF),
         vm((ROWS, HEADS), F32), vm((HEADS, ROWS), F32), vm((ROWS, HEADS), F32), vm((HEADS, ROWS), F32),
         vm((ROWS, INNER), F32), vm((NB, STATE, INNER), F32), vm((STATE, INNER), BF), vm((STATE, INNER), BF),
-        vm((8, 128), F32), vm((N, 8, 128), F32), vm((8, 128), F32), vm((N, 8, 128), F32),
+        vm((1, 128), F32), vm((N, 1, 128), F32), vm((1, 128), F32), vm((N, 1, 128), F32),
         vm((N, SLICE, INNER), F32), vm((N, SLICE, INNER), BF), vm((SLICE, INNER), BF), vm((N, SLICE, INNER), BF),
         vm((N, SLICE, INNER), BF),
         vm((ROWS, INNER), BF), vm((INNER, D), BF), vm((N, N, PIECE, FF), BF), vm((N, N, PIECE, FF), BF),

time: 80.7 us -> 79.6 us (0.986)
  Pallas kernels: 79.9 us -> 78.8 us
    pallas_call x1, Pallas kernels: 79.9 us -> 78.8 us  [shards(): pl.pallas_call(kernel, out_shape=pltpu.VMEM((ROWS, COLS), BF), in_specs=[...]
where the time goes in v4:
time: 79.6 us; the launch traced here: 79.5 us
  Pallas kernels  78.8 us (99%)
    pallas_call x1, Pallas kernels, shards(): pl.pallas_call(kernel, out_shape=pltpu.VMEM((ROWS, COLS), BF), in_specs=[...  78.8 us

profile of v4, /device:TPU:1, one launch (start us, length us, event | category | flops | bytes accessed | tf_op | source)
XLA Modules:
  0.0 79.5 jit_solution(15221705061382548153)
XLA Ops:
  0.0 78.8 %layer.1 = bf16[384,256]{1,0:T(8,128)(2,1)S(1)} custom-call(bf16[384,512]{1,0:T(8,128)(2,1)} %inner_hbm.1, bf16[384,2,128]{2,1,0:T(2,128)(2,1)} %coeff_hbm.1, bf16[384,512]{1,0:T(8,128)(2,1)} %gate_hbm.1, bf16[8,384]{1,0:T(8,128)(2,1)} %bitcast.7, f32[1,8]{1,0:T(1,128)} %bitcast.10, f32[1,8]{1,0:T(1,128)} %bitcast.11, bf16[4,512]{1,0:T(4,128)(2,1)} %taps_inner_hbm.1, ...), custom_call_target="tpu_custom_call" | custom-call | tf_op jit(solution)/shard_map/layer/pallas_call | solution.py:585
  78.8 0.7 copy.16

commit v5 on v4

--- a/solution.py
+++ b/solution.py
@@ -56,7 +56,7 @@
     hist_inner, hist_coeff, ext, ext_c, act, cum, cum_t, step, step_t, local, states, own, enter,
     ld_own, ld_row, ld_total, ld_rows, pre, st_row, st_total, st_rows, st_back,
     mixed, out_w, up_all, down_all, gain_own, gain_all,
-    rows, first, acc, active, send, recv, local_sem, *reductions,
+    rows, first, acc, active, send, recv, local_sem, tokens, *reductions,
 ):
     z, y, x, c = (lax.axis_index(a) for a in ("z", "y", "x", "c"))
     tp = 2 * x + c
@@ -69,9 +69,8 @@
     tp_id = lambda d: {"x": at(tp, d) // 2, "c": lax.rem(at(tp, d), 2)}
 
     barrier = pltpu.get_barrier_semaphore()
-    greeted = [next_id, prev_id]
-    for d in range(1, N):
-        greeted += [{"y": at(y, d)}, {"z": at(z, d)}, tp_id(d)]
+    beside = [{"y": at(y, 1)}, {"y": at(y, N - 1)}, {"z": at(z, 1)}, {"z": at(z, N - 1)}]
+    greeted = beside + [right, left, partner, next_id, prev_id]
     for where in greeted:
         pl.semaphore_signal(barrier, inc=1, device_id=where, device_id_type=MESH)
 
@@ -79,16 +78,16 @@
         pltpu.make_async_copy(there, here, local_sem.at[i])
         for i, (there, here) in enumerate(
             (
-                (step_raw_hbm, step_raw), (step_bias_hbm, step_bias), (decay_log_hbm, decay_log),
-                (mlp_gain_hbm, mlp_gain), (taps_inner_hbm, taps_inner), (taps_coeff_hbm, taps_coeff),
-                (up_hbm, up), (down_hbm, down), (inner_hbm, inner), (coeff_hbm, coeff),
-                (mixer_gain_hbm, mixer_gain), (gate_hbm, gate), (residual_hbm, residual), (out_hbm, out_w),
+                (up_hbm, up), (down_hbm, down), (inner_hbm, inner), (coeff_hbm, coeff), (step_raw_hbm, step_raw),
+                (step_bias_hbm, step_bias), (decay_log_hbm, decay_log), (mlp_gain_hbm, mlp_gain),
+                (taps_inner_hbm, taps_inner), (taps_coeff_hbm, taps_coeff), (mixer_gain_hbm, mixer_gain),
+                (gate_hbm, gate), (residual_hbm, residual), (out_hbm, out_w),
             )
         )
     ]
     for copy in fetched:
         copy.start()
-    up_copy, down_copy, inner_copy, coeff_copy, mixer_gain_copy, gate_copy, residual_copy, out_copy = fetched[6:]
+    mixer_gain_copy, gate_copy, residual_copy, out_copy = fetched[10:]
 
     used = [0, 0]
     pending = []
@@ -121,36 +120,6 @@
     eye = (row_i == col_i).astype(F32)
     low_lanes = col_i < 64
 
-    on_heads = lax.broadcasted_iota(jnp.int32, (HEADS, HEADS), 0) == lax.broadcasted_iota(jnp.int32, (HEADS, HEADS), 1)
-    column = lambda v: jnp.sum(jnp.where(on_heads, jnp.broadcast_to(v, (HEADS, HEADS)), 0.0), axis=1, keepdims=True)
-    for copy in fetched[:6]:
-        copy.wait()
-    bias = column(step_bias[...])
-    rate = jnp.exp(column(decay_log[...]))
-    ends = []
-    for b in range(NB):
-        rb = pl.ds(b * BLOCK, BLOCK)
-        raw = step_raw[:, rb].astype(F32) + bias
-        size = jnp.maximum(raw, 0.0) + jnp.log1p(jnp.exp(-jnp.abs(raw)))
-        logs = -size * rate
-        cum_b = dot(tril, logs, NT, HIGH)
-        cum[rb, :] = cum_b
-        cum_t[:, rb] = dot(logs, triu, NN, HIGH)
-        step[rb, :] = dot(eye, size, NT, HIGH)
-        step_t[:, rb] = size
-        ends.append(cum_b[BLOCK - 1 : BLOCK, :])
-    total = ends[0] + ends[1] + ends[2]
-    ld_own[...] = jnp.zeros_like(ld_own)
-    ld_own[:, 0:HEADS] = total
-    gain_own[...] = jnp.broadcast_to(mlp_gain[...], gain_own.shape)
-
-    pl.semaphore_wait(barrier, len(greeted))
-
-    inner_copy.wait()
-    coeff_copy.wait()
-    inner_tail, coeff_tail = receiver(), receiver()
-    go(inner.at[pl.ds(ROWS - EDGE, EDGE)], hist_inner, next_id, sender(hist_inner), inner_tail)
-    go(coeff.at[pl.ds(ROWS - 8, 8)], hist_coeff, next_id, sender(hist_coeff), coeff_tail)
     seven = pl.ds(0, N - 1)
 
     def to_all(source, target, where):
@@ -160,13 +129,6 @@
         return lambda: landed(arrived, target[1])
 
     along_y, along_z = lambda d: {"y": at(y, d)}, lambda d: {"z": at(z, d)}
-    ld_landed = to_all(lambda d: ld_own, (ld_row.at[y], ld_row.at[seven]), along_y)
-    gain_landed = to_all(lambda d: gain_own, (gain_all.at[tp], gain_all.at[seven]), tp_id)
-    ld_row[y] = ld_own[...]
-    gain_all[tp] = gain_own[...]
-
-    up_copy.wait()
-    down_copy.wait()
     OFFSETS = ((0,), (N - 1, 1), (N - 2, 2), (N - 3, 3), (4,))
     weights_sent = [[sender(w.at[0, seven]), sender(w.at[seven])] for w in (up_all, down_all)]
     weights_landed = [
@@ -259,10 +221,51 @@
     def fill(k):
         rounds(1, DOWN[k])
 
+    for copy in fetched[:4]:
+        copy.wait()
+    pl.semaphore_wait(barrier, len(greeted))
+    inner_tail, coeff_tail = receiver(), receiver()
+    go(inner.at[pl.ds(ROWS - EDGE, EDGE)], hist_inner, next_id, sender(hist_inner), inner_tail)
+    go(coeff.at[pl.ds(ROWS - 8, 8)], hist_coeff, next_id, sender(hist_coeff), coeff_tail)
     event(0)
     fill(0)
+
+    def pass_tokens(first, targets):
+        for i, where in enumerate(targets):
+            pl.semaphore_signal(tokens.at[first + i], inc=1, device_id=where, device_id_type=MESH)
+
+    def take_tokens(first):
+        for i in range(4):
+            pl.semaphore_wait(tokens.at[first + i], 1)
+
+    pass_tokens(0, beside)
+    pl.semaphore_signal(tokens.at[4], inc=1, device_id=right, device_id_type=MESH)
+    pl.semaphore_signal(tokens.at[5], inc=1, device_id=left, device_id_type=MESH)
     up_all[z, y] = up[...]
     down_all[z, y] = down[...]
+
+    on_heads = lax.broadcasted_iota(jnp.int32, (HEADS, HEADS), 0) == lax.broadcasted_iota(jnp.int32, (HEADS, HEADS), 1)
+    column = lambda v: jnp.sum(jnp.where(on_heads, jnp.broadcast_to(v, (HEADS, HEADS)), 0.0), axis=1, keepdims=True)
+    for copy in fetched[4:10]:
+        copy.wait()
+    bias = column(step_bias[...])
+    rate = jnp.exp(column(decay_log[...]))
+    ends = []
+    for b in range(NB):
+        rb = pl.ds(b * BLOCK, BLOCK)
+        raw = step_raw[:, rb].astype(F32) + bias
+        size = jnp.maximum(raw, 0.0) + jnp.log1p(jnp.exp(-jnp.abs(raw)))
+        logs = -size * rate
+        cum_b = dot(tril, logs, NT, HIGH)
+        cum[rb, :] = cum_b
+        cum_t[:, rb] = dot(logs, triu, NN, HIGH)
+        step[rb, :] = dot(eye, size, NT, HIGH)
+        step_t[:, rb] = size
+        ends.append(cum_b[BLOCK - 1 : BLOCK, :])
+    total = ends[0] + ends[1] + ends[2]
+    ld_own[...] = jnp.zeros_like(ld_own)
+    ld_own[:, 0:HEADS] = total
+    gain_own[...] = jnp.broadcast_to(mlp_gain[...], gain_own.shape)
 
     ext[8 : 8 + ROWS, :] = inner[...].astype(F32)
     ext_c[8 : 8 + ROWS] = coeff[...].astype(F32)
@@ -293,8 +296,13 @@
         states[b] = dot(act[rb, INNER : INNER + STATE], values.astype(BF), TN)
 
     taps(1)
+    block_state(1)
+    take_tokens(0)
+    pass_tokens(7, [{"y": at(y, 2)}, {"y": at(y, N - 2)}, {"z": at(z, 2)}, {"z": at(z, N - 2)}])
+    pl.semaphore_wait(tokens.at[4], 1)
+    pl.semaphore_wait(tokens.at[5], 1)
+    pl.semaphore_signal(tokens.at[6], inc=1, device_id=partner, device_id_type=MESH)
     taps(2)
-    block_state(1)
     block_state(2)
     taps(0)
     landed(inner_tail, hist_inner)
@@ -309,6 +317,10 @@
     ).astype(BF)
 
     slice_of = lambda v: pl.ds(pl.multiple_of(v * SLICE, SLICE), SLICE)
+    take_tokens(7)
+    pl.semaphore_wait(tokens.at[6], 1)
+    ld_landed = to_all(lambda d: ld_own, (ld_row.at[y], ld_row.at[seven]), along_y)
+    ld_row[y] = ld_own[...]
     st1_landed = to_all(lambda d: own.at[slice_of(at(y, d))], (st_row.at[y], st_row.at[seven]), along_y)
     event(1)
     fill(1)
@@ -334,6 +346,8 @@
             inner_state = states[0] * per_head(jnp.exp(ends[1])) + states[1]
         local[rb, :] += dot(act[rb, INNER + STATE :], inner_state.astype(BF), NN) * per_head(jnp.exp(cum[rb, :]))
 
+    gain_landed = to_all(lambda d: gain_own, (gain_all.at[tp], gain_all.at[seven]), tp_id)
+    gain_all[tp] = gain_own[...]
     ld_landed()
     row_logs = ld_row[:, 0, :]
     ld_total[...] = jnp.sum(row_logs, axis=0, keepdims=True)
@@ -575,7 +589,7 @@
         vm((ROWS, INNER), BF), vm((INNER, D), BF), vm((N, N, PIECE, FF), BF), vm((N, N, PIECE, FF), BF),
         vm((8, COLS), F32), vm((N, 8, COLS), F32),
         vm((N, ROWS, COLS), BF), vm((ROWS, COLS), BF), vm((ROWS, FF), F32), vm((ROWS, FF), BF),
-        dma((19,)), dma((83,)), dma((14,)),
+        dma((19,)), dma((83,)), dma((14,)), pltpu.SemaphoreType.REGULAR((11,)),
     ]
     for width in (COLS, COLS // 2, COLS // 2):
         scratch += [

time: 79.6 us -> 79.2 us (level)
  no operation moved by 1% of the time
where the time goes in v5:
time: 79.2 us; the launch traced here: 79.1 us
  Pallas kernels  78.4 us (99%)
    pallas_call x1, Pallas kernels, shards(): pl.pallas_call(kernel, out_shape=pltpu.VMEM((ROWS, COLS), BF), in_specs=[...  78.4 us

profile of v5, /device:TPU:1, one launch (start us, length us, event | category | flops | bytes accessed | tf_op | source)
XLA Modules:
  0.0 79.1 jit_solution(1990894291025717705)
XLA Ops:
  0.0 78.4 %layer.1 = bf16[384,256]{1,0:T(8,128)(2,1)S(1)} custom-call(bf16[384,512]{1,0:T(8,128)(2,1)} %inner_hbm.1, bf16[384,2,128]{2,1,0:T(2,128)(2,1)} %coeff_hbm.1, bf16[384,512]{1,0:T(8,128)(2,1)} %gate_hbm.1, bf16[8,384]{1,0:T(8,128)(2,1)} %bitcast.7, f32[1,8]{1,0:T(1,128)} %bitcast.10, f32[1,8]{1,0:T(1,128)} %bitcast.11, bf16[4,512]{1,0:T(4,128)(2,1)} %taps_inner_hbm.1, ...), custom_call_target="tpu_custom_call" | custom-call | tf_op jit(solution)/shard_map/layer/pallas_call | solution.py:599
  78.4 0.7 copy.16
